TPU v7x, 256 devices: a 8x8x2 block of a 8x8x16 slice. The times are simulated.
256 devices in a mesh: grp: 2 (over z), st: 16 (over y, core), tp: 8 (over x).
Axes of the slice: x: 8, y: 8, z: 2, core: 2. Of those that a mesh axis runs over, the one named last changes fastest.
The devices are a block of a 8x8x16 slice.
Arguments:
- tokens: bfloat16 [8192, 2048], P(('grp', 'st')), parts along dimension 0, may hold values from -6 to 6
- pre_gain: float32 [2048], replicated, may hold values from 0.1 to 1.9
- w_gated: bfloat16 [2048, 1536], P(None, 'tp'), may hold values from -0.125 to 0.125
- w_mixed: bfloat16 [2048, 1536], P(None, 'tp'), may hold values from -0.125 to 0.125
- mix_weight: bfloat16 [8, 128, 128], P('tp'), may hold values from -0.5 to 0.5
- w_query: bfloat16 [2048, 1024], P(None, 'tp'), may hold values from -0.125 to 0.125
- w_gate_mix: bfloat16 [2048, 1536], P(None, 'tp'), may hold values from -0.125 to 0.125
- w_gate_read: bfloat16 [2048, 1024], P(None, 'tp'), may hold values from -0.125 to 0.125
- store: bfloat16 [256, 128, 2048], P(('grp', 'st')), parts along dimension 0, may hold values from -6 to 6
- mem_gain: float32 [2048], replicated, may hold values from 1 to 80
- w_key: bfloat16 [2048, 1024], P(None, 'tp'), may hold values from -0.125 to 0.125
- w_value: bfloat16 [2048, 1024], P(None, 'tp'), may hold values from -0.125 to 0.125
- passage_ids: int32 [128, 4], P(('grp', 'st')), parts along dimension 0, may hold values from 0 to 127, as said below
- w_out_mix: bfloat16 [1536, 2048], P('tp'), may hold values from -0.125 to 0.125
- w_out_read: bfloat16 [1024, 2048], P('tp'), may hold values from -0.125 to 0.125
Outputs:
- mixed_out: bfloat16 [8192, 2048], P(('grp', 'st', 'tp')), parts along dimension 0
There are 2 independent parts, one for each index of `grp`. A program takes and returns all parts, laid end to end along the dimension named above; an argument that names none is the same for every part. Nothing has to cross between parts.
Inputs may be any that keep to these rules, and one draw needn't show every extreme that they name: `passage_ids`: passage p is held by index p // 8 of st. The 16 entries of one index of st name at most 2 passages held by any one index of st, and that most is reached in every draw.
All inputs are finite; a program needn't handle non-finite values.
Results may differ from a plain program's by a relative error of at most 0.015.
The roundings to bfloat16 on the way count: a program that leaves them out, or rounds other values in their place, can miss the bound.
Values may be sent and summed in bfloat16 or wider, within the bound.
A program may use at most 128 MiB of HBM per device.

v0:
```python
import jax
import jax.numpy as jnp
from jax import lax
from jax.sharding import PartitionSpec as P

HD = 128
SPAN = 128
RBLOCK = 64
NPB = 4
PROWS = 128


eps = 1e-06


def split_up(x, dim, size):
    lengths = x.shape
    parts = x.reshape(*lengths[:dim], size, lengths[dim] // size, *lengths[dim + 1 :])
    return jnp.moveaxis(parts, dim, 0)


def summed_on_arrival(x, axis, dim):
    parts = split_up(x, dim, lax.axis_size(axis))
    arrived = lax.all_to_all(parts, axis, split_axis=0, concat_axis=0, tiled=True)
    return arrived.astype(jnp.float32).sum(axis=0)


def row_norm(values_in, gain):
    widened = values_in.astype(jnp.float32)
    return (
        widened * lax.rsqrt(jnp.mean(widened * widened, axis=-1, keepdims=True) + eps) * gain
    ).astype(jnp.bfloat16)


def local(
    tokens,
    pre_gain,
    w_gated,
    w_mixed,
    mix_weight,
    w_query,
    w_gate_mix,
    w_gate_read,
    store,
    mem_gain,
    w_key,
    w_value,
    passage_ids,
    w_out_mix,
    w_out_read,
):
    tok_rows = tokens.shape[0]
    st_count = lax.axis_size("st")
    normed = row_norm(tokens, pre_gain)
    gated = jnp.dot(normed, w_gated, preferred_element_type=jnp.float32)
    mixed_in = jnp.dot(normed, w_mixed, preferred_element_type=jnp.float32)
    groups_here = mix_weight.shape[0]
    group_width = mixed_in.shape[1] // groups_here
    grouped = mixed_in.reshape(tok_rows, groups_here, group_width)
    group_mean = jnp.mean(grouped, axis=-1, keepdims=True)
    centred = grouped - group_mean
    group_var = jnp.mean(centred * centred, axis=-1, keepdims=True)
    mixed_norm = (centred * lax.rsqrt(group_var + eps)).astype(jnp.bfloat16)
    causal = jnp.tril(jnp.ones((SPAN, SPAN), dtype=bool))
    mix_masked = jnp.where(causal[None], mix_weight, jnp.zeros_like(mix_weight))
    blocked = mixed_norm.reshape(tok_rows // SPAN, SPAN, groups_here, group_width)
    spatial = jnp.einsum(
        "hts,nshd->nthd", mix_masked, blocked, preferred_element_type=jnp.float32
    ).reshape(tok_rows, -1)
    branch_mix = gated * spatial
    query = jnp.dot(normed, w_query, preferred_element_type=jnp.float32).astype(jnp.bfloat16)
    head_width = w_query.shape[1]
    heads_here = head_width // HD
    flat_ids = passage_ids.reshape(-1)
    req_count = flat_ids.shape[0]
    per_owner = store.shape[0]
    capacity = max(2, (2 * req_count + st_count - 1) // st_count)
    owner = flat_ids // per_owner
    local_id = flat_ids - owner * per_owner
    position = jnp.arange(req_count, dtype=jnp.int32)
    same_owner = owner[:, None] == owner[None, :]
    earlier = position[None, :] < position[:, None]
    rank = jnp.sum((same_owner & earlier).astype(jnp.int32), axis=1)
    slot = owner * capacity + rank
    slot_range = jnp.arange(st_count * capacity, dtype=jnp.int32)
    table = jnp.sum(jnp.where(slot[:, None] == slot_range[None, :], local_id[:, None], 0), axis=0)
    table = table.reshape(st_count, capacity)
    held_rows = row_norm(store, mem_gain).reshape(-1, store.shape[-1])
    key_store = (
        jnp.dot(held_rows, w_key, preferred_element_type=jnp.float32)
        .astype(jnp.bfloat16)
        .reshape(per_owner, PROWS, head_width)
    )
    value_store = (
        jnp.dot(held_rows, w_value, preferred_element_type=jnp.float32)
        .astype(jnp.bfloat16)
        .reshape(per_owner, PROWS, head_width)
    )
    wanted = lax.all_to_all(table, "st", split_axis=0, concat_axis=0, tiled=True)
    arrived = (
        lax.all_to_all(key_store[wanted], "st", split_axis=0, concat_axis=0, tiled=True),
        lax.all_to_all(value_store[wanted], "st", split_axis=0, concat_axis=0, tiled=True),
    )
    blocks_here = tok_rows // RBLOCK
    key_slots, value_slots = arrived
    keys = key_slots.reshape(st_count * capacity, PROWS, head_width)[slot]
    values = value_slots.reshape(st_count * capacity, PROWS, head_width)[slot]
    keys = keys.reshape(blocks_here, NPB * PROWS, heads_here, HD)
    values = values.reshape(blocks_here, NPB * PROWS, heads_here, HD)
    query_blocks = query.reshape(blocks_here, RBLOCK, heads_here, HD)
    scores = jnp.einsum(
        "btha,bkha->bhtk", query_blocks, keys, preferred_element_type=jnp.float32
    ) * HD ** (-0.5)
    probs = jax.nn.softmax(scores, axis=-1).astype(jnp.bfloat16)
    branch_read = jnp.einsum(
        "bhtk,bkha->btha", probs, values, preferred_element_type=jnp.float32
    ).reshape(tok_rows, head_width)
    gate_mix = jnp.dot(normed, w_gate_mix, preferred_element_type=jnp.float32)
    gate_read = jnp.dot(normed, w_gate_read, preferred_element_type=jnp.float32)
    out_mix = (branch_mix * jax.nn.silu(gate_mix)).astype(jnp.bfloat16)
    out_read = (branch_read * jax.nn.silu(gate_read)).astype(jnp.bfloat16)
    summed = summed_on_arrival(
        (
            jnp.dot(out_mix, w_out_mix, preferred_element_type=jnp.float32)
            + jnp.dot(out_read, w_out_read, preferred_element_type=jnp.float32)
        ).astype(jnp.bfloat16),
        "tp",
        0,
    )
    return summed.astype(jnp.bfloat16)


def solution(mesh):
    placed = (
        P(("grp", "st"), None),
        P(),
        P(None, "tp"),
        P(None, "tp"),
        P("tp", None, None),
        P(None, "tp"),
        P(None, "tp"),
        P(None, "tp"),
        P(("grp", "st"), None, None),
        P(),
        P(None, "tp"),
        P(None, "tp"),
        P(("grp", "st"), None),
        P("tp", None),
        P("tp", None),
    )
    return jax.shard_map(
        local, mesh=mesh, in_specs=placed, out_specs=P(("grp", "st", "tp"), None), check_vma=False
    )
```

profile of v0, /device:TPU:513, one launch (start us, length us, event | category | flops | bytes accessed | tf_op | source)
XLA Modules:
  0.0 140.8 jit_solution(3696719735241878890)
XLA Ops:
  0.0 0.0 copy-start
  0.0 0.8 reshape.317
  0.9 0.2 convert_reduce_fusion
  1.0 0.1 select_reduce_fusion
  1.1 0.7 all_to_all.17
  1.8 23.7 %all-to-all-start = ((s32[16,1,2]{2,1,0:T(1,128)}), s32[16,1,2]{2,1,0:T(1,128)S(1)}, u32[]{:S(2)}, u32[]{:S(2)}) async-start(s32[16,1,2]{2,1,0:T(1,128)} %bitcast.6), calls=%async_computation | async-start | bytes 16384 | tf_op jit(solution)/shard_map/all_to_all | solution.py:99
  25.5 0.0 copy-start.7
  25.5 3.2 %fusion.1 = f32[8,128]{1,0:T(8,128)S(1)} fusion(bf16[8,128,2048]{2,1,0:T(8,128)(2,1)} %param.23), kind=kLoop, calls=%fused_computation.7 | loop fusion | flops 6290432 | bytes 4198400 | tf_op jit(solution)/shard_map/reduce_sum | solution.py:31
  28.8 0.2 copy-done.1
  29.0 0.0 copy-done.7
  29.0 1.0 fusion.3
  30.0 0.0 copy-start.2
  30.0 1.9 %copy-done.2 = bf16[8,128,2048]{2,1,0:T(8,128)(2,1)} copy-done((bf16[8,128,2048]{2,1,0:T(8,128)(2,1)}, bf16[8,128,2048]{2,1,0:T(8,128)(2,1)S(1)}, u32[]{:S(2)}) %copy-start.2) | copy-done | bytes 4194328
  31.9 1.2 convolution_convert_fusion
  33.2 0.0 all-to-all-done
  33.2 0.1 copy.31
  33.3 0.1 copy.32
  33.4 0.1 reshape.329
  33.5 0.0 copy-start.9
  33.5 0.0 copy-start.3
  33.5 1.7 %gather_fusion.2 = bf16[32,128,128]{2,1,0:T(8,128)(2,1)} fusion(bf16[8,128,128]{2,1,0:T(8,128)(2,1)S(1)} %bitcast.74, s32[1024]{0:T(1024)S(1)} %pad_clamp_fusion.1), kind=kCustom, calls=%fused_computation.2 | custom fusion | bytes 2097280 | tf_op jit(solution)/shard_map/gather | solution.py:101
  35.2 7.5 %all-to-all-start.2 = ((bf16[16,2,128,128]{3,2,1,0:T(8,128)(2,1)}), bf16[16,2,128,128]{3,2,1,0:T(8,128)(2,1)S(1)}, u32[]{:S(2)}, u32[]{:S(2)}) async-start(bf16[16,2,128,128]{3,2,1,0:T(8,128)(2,1)} %bitcast.15), calls=%async_computation.2 | async-start | bytes 2097152 | tf_op jit(solution)/shard_map/all_to_all | solution.py:101
  42.7 0.1 reshape.319
  42.7 0.3 fusion.5
  43.1 1.7 %fusion.46 = (f32[256]{0:T(256)S(1)}, f32[256,192]{0,1:T(8,128)S(1)}) fusion(bf16[2048,192]{0,1:T(8,128)(2,1)} %param.18, bf16[256,2048]{1,0:T(8,128)(2,1)S(1)} %copy-done.3, f32[2048]{0:T(1024)S(1)} %copy-done.8, f32[256]{0:T(256)S(1)} %add_rsqrt_fusion.2), kind=kOutput, calls=%fused_computation.80 | convolution fusion | flops 203472640 | bytes 2041856 | tf_op jit(solution)/shard_map/dot_general | solution.py:56
  44.8 3.4 %convolution_convert_fusion.1 = bf16[1024,128]{1,0:T(8,128)(2,1)S(1)} fusion(bf16[1024,2048]{1,0:T(8,128)(2,1)} %bitcast.73, bf16[2048,128]{1,0:T(8,128)(2,1)S(1)} %copy-done.12), kind=kOutput, calls=%fused_computation.21 | convolution fusion | flops 537001984 | bytes 4980736 | tf_op jit(solution)/shard_map/dot_general | solution.py:95
  48.3 0.0 copy-start.6
  48.3 1.7 %gather_fusion = bf16[32,128,128]{2,1,0:T(8,128)(2,1)} fusion(bf16[8,128,128]{2,1,0:T(8,128)(2,1)S(1)} %bitcast.75, s32[1024]{0:T(1024)S(1)} %pad_clamp_fusion.1), kind=kCustom, calls=%fused_computation | custom fusion | bytes 2097280 | tf_op jit(solution)/shard_map/gather | solution.py:102
  50.0 20.7 %all-to-all-done.2 = bf16[16,2,128,128]{3,2,1,0:T(8,128)(2,1)S(1)} async-done(((bf16[16,2,128,128]{3,2,1,0:T(8,128)(2,1)}), bf16[16,2,128,128]{3,2,1,0:T(8,128)(2,1)S(1)}, u32[]{:S(2)}, u32[]{:S(2)}) %all-to-all-start.2) | async-done | bytes 1048608 | tf_op jit(solution)/shard_map/all_to_all | solution.py:101
  70.6 4.4 %all-to-all-start.1 = ((bf16[16,2,128,128]{3,2,1,0:T(8,128)(2,1)}), bf16[16,2,128,128]{3,2,1,0:T(8,128)(2,1)}, u32[]{:S(2)}, u32[]{:S(2)}) async-start(bf16[16,2,128,128]{3,2,1,0:T(8,128)(2,1)} %bitcast.8), calls=%async_computation.1 | async-start | bytes 2097152 | tf_op jit(solution)/shard_map/all_to_all | solution.py:102
  75.1 0.0 copy-start.10
  75.1 0.0 copy-done.6
  75.1 0.2 convolution_bitcast_fusion
  75.3 0.2 copy.29
  75.5 2.2 %convolution_convert_fusion.2 = bf16[256,128]{1,0:T(8,128)(2,1)} fusion(bf16[2048,128]{1,0:T(8,128)(2,1)} %param.20, bf16[256,2048]{1,0:T(8,128)(2,1)S(1)} %copy-done.3, f32[2048]{0:T(1024)S(1)} %copy-done.8, f32[256]{0:T(256)S(1)} %add_rsqrt_fusion.2), kind=kOutput, calls=%fused_computation.27 | convolution fusion | flops 136347648 | bytes 1647616 | tf_op jit(solution)/shard_map/dot_general | solution.py:71
  77.7 0.6 fusion.38
  78.3 3.0 %fusion.12 = f32[256,2048]{1,0:T(8,128)S(1)} fusion(bf16[192,2048]{1,0:T(8,128)(2,1)S(1)} %copy-done, bf16[2048,192]{0,1:T(8,128)(2,1)} %param.17, f32[24,8,2,128]{3,2,1,0:T(2,128)S(1)} %bitcast.78, f32[256,192]{0,1:T(8,128)S(1)} %fusion.38, bf16[256,2048]{1,0:T(8,128)(2,1)} %param.15, f32[2048]{0:T(1024)S(1)} %copy-done.8, f32[256]{0:T(256)S(1)} %add_rsqrt_fusion.2), kind=kOutput, calls=%fused_computation.26 | convolution fusion | flops 405094400 | bytes 5121024 | tf_op jit(solution)/shard_map/dot_general | solution.py:124
  81.2 2.6 %gather_fusion.3 = bf16[16,128,128]{2,1,0:T(8,128)(2,1)} fusion(bf16[32,128,128]{2,1,0:T(8,128)(2,1)} %bitcast.76, s32[1024]{0:T(1024)S(1)} %pad_clamp_fusion), kind=kCustom, calls=%fused_computation.3 | custom fusion | bytes 1048640 | tf_op jit(solution)/shard_map/gather | solution.py:106
  83.9 1.4 convolution_multiply_fusion
  85.2 0.2 fusion.47
  85.5 16.7 %all-to-all-done.1 = bf16[16,2,128,128]{3,2,1,0:T(8,128)(2,1)} async-done(((bf16[16,2,128,128]{3,2,1,0:T(8,128)(2,1)}), bf16[16,2,128,128]{3,2,1,0:T(8,128)(2,1)}, u32[]{:S(2)}, u32[]{:S(2)}) %all-to-all-start.1) | async-done | bytes 1048608 | tf_op jit(solution)/shard_map/all_to_all | solution.py:102
  102.1 2.6 %gather_fusion.1 = bf16[16,128,128]{2,1,0:T(8,128)(2,1)} fusion(bf16[32,128,128]{2,1,0:T(8,128)(2,1)} %bitcast.9, s32[1024]{0:T(1024)S(1)} %pad_clamp_fusion), kind=kCustom, calls=%fused_computation.1 | custom fusion | bytes 1048640 | tf_op jit(solution)/shard_map/gather | solution.py:107
  104.8 2.3 %fusion.13 = f32[4,128,64]{1,2,0:T(8,128)} fusion(bf16[4,512,128]{2,1,0:T(8,128)(2,1)} %bitcast.79, f32[4,64]{1,0:T(4,128)S(1)} %fusion.47, f32[4,64,512]{2,1,0:T(8,128)S(1)} %convolution_multiply_fusion), kind=kOutput, calls=%fused_computation.29 | convolution fusion | flops 33948416 | bytes 1180672 | tf_op jit(solution)/shard_map/bhtk,bkha->btha/dot_general | solution.py:115
  107.0 2.0 %fusion.21 = bf16[256,128]{1,0:T(8,128)(2,1)S(1)} fusion(f32[4,128,64]{1,2,0:T(8,128)} %fusion.13, bf16[2048,128]{1,0:T(8,128)(2,1)} %param.22, bf16[256,2048]{1,0:T(8,128)(2,1)} %param.15, f32[2048]{0:T(1024)S(1)} %copy-done.8, f32[256]{0:T(256)S(1)} %add_rsqrt_fusion.2), kind=kOutput, calls=%fused_computation.40 | convolution fusion | flops 136511488 | bytes 1778688 | tf_op jit(solution)/shard_map/dot_general | solution.py:119
  109.0 0.0 copy-done.5
  109.0 0.4 fusion.4
  109.4 30.6 %all_to_all.27 = bf16[8,32,2048]{2,1,0:T(8,128)(2,1)S(1)} all-to-all(bf16[8,32,2048]{2,1,0:T(8,128)(2,1)S(1)} %bitcast.71), channel_id=1, replica_groups=mesh['grp'=2,'st'=16,'tp'=8] {'tp'}, dimensions={0} | all-to-all | bytes 2097152 | tf_op jit(solution)/shard_map/all_to_all | solution.py:24
  140.0 0.8 reduce_sum.85
  (25 shorter events, 0.2 us)
Async XLA Ops:
  0.0 78.3 %copy-start = (bf16[192,2048]{1,0:T(8,128)(2,1)S(1)}, bf16[192,2048]{1,0:T(8,128)(2,1)}, u32[]{:S(2)}) copy-start(bf16[192,2048]{1,0:T(8,128)(2,1)} %param.28) | copy-start | bytes 2359300
  1.8 31.4 %all-to-all-start = ((s32[16,1,2]{2,1,0:T(1,128)}), s32[16,1,2]{2,1,0:T(1,128)S(1)}, u32[]{:S(2)}, u32[]{:S(2)}) async-start(s32[16,1,2]{2,1,0:T(1,128)} %bitcast.6), calls=%async_computation | async-start | bytes 16384 | tf_op jit(solution)/shard_map/all_to_all | solution.py:99
  25.5 3.4 %copy-start.1 = (bf16[8,128,2048]{2,1,0:T(8,128)(2,1)S(1)}, bf16[8,128,2048]{2,1,0:T(8,128)(2,1)}, u32[]{:S(2)}) copy-start(bf16[8,128,2048]{2,1,0:T(8,128)(2,1)} %param.23) | copy-start | bytes 12582916
  25.5 3.4 %copy-start.7 = (f32[2048]{0:T(1024)S(1)}, f32[2048]{0:T(1024)}, u32[]{:S(2)}) copy-start(f32[2048]{0:T(1024)} %param.24) | copy-start | bytes 24580
  29.0 3.0 %copy-start.11 = (bf16[2048,128]{1,0:T(8,128)(2,1)S(1)}, bf16[2048,128]{1,0:T(8,128)(2,1)}, u32[]{:S(2)}) copy-start(bf16[2048,128]{1,0:T(8,128)(2,1)} %param.25) | copy-start | bytes 1572868
  30.0 1.9 %copy-start.2 = (bf16[8,128,2048]{2,1,0:T(8,128)(2,1)}, bf16[8,128,2048]{2,1,0:T(8,128)(2,1)S(1)}, u32[]{:S(2)}) copy-start(bf16[8,128,2048]{2,1,0:T(8,128)(2,1)S(1)} %fusion.3) | copy-start | bytes 12582916
  33.5 9.2 %copy-start.9 = (s32[4,4]{1,0:T(4,128)S(1)}, s32[4,4]{1,0:T(4,128)}, u32[]{:S(2)}) copy-start(s32[4,4]{1,0:T(4,128)} %param.27) | copy-start | bytes 196
  33.5 9.3 %copy-start.3 = (bf16[256,2048]{1,0:T(8,128)(2,1)S(1)}, bf16[256,2048]{1,0:T(8,128)(2,1)}, u32[]{:S(2)}) copy-start(bf16[256,2048]{1,0:T(8,128)(2,1)} %param.15) | copy-start | bytes 3145732
  35.1 7.9 %copy-start.8 = (f32[2048]{0:T(1024)S(1)}, f32[2048]{0:T(1024)}, u32[]{:S(2)}) copy-start(f32[2048]{0:T(1024)} %param.16) | copy-start | bytes 24580
  35.2 35.5 %all-to-all-start.2 = ((bf16[16,2,128,128]{3,2,1,0:T(8,128)(2,1)}), bf16[16,2,128,128]{3,2,1,0:T(8,128)(2,1)S(1)}, u32[]{:S(2)}, u32[]{:S(2)}) async-start(bf16[16,2,128,128]{3,2,1,0:T(8,128)(2,1)} %bitcast.15), calls=%async_computation.2 | async-start | bytes 2097152 | tf_op jit(solution)/shard_map/all_to_all | solution.py:101
  42.7 2.1 %copy-start.12 = (bf16[2048,128]{1,0:T(8,128)(2,1)S(1)}, bf16[2048,128]{1,0:T(8,128)(2,1)}, u32[]{:S(2)}) copy-start(bf16[2048,128]{1,0:T(8,128)(2,1)} %param.26) | copy-start | bytes 1572868
  48.3 26.8 %copy-start.6 = (bf16[1,128,128]{2,1,0:T(8,128)(2,1)S(1)}, bf16[1,128,128]{2,1,0:T(8,128)(2,1)}, u32[]{:S(2)}) copy-start(bf16[1,128,128]{2,1,0:T(8,128)(2,1)} %param.19) | copy-start | bytes 98308
  70.6 7.0 %copy-start.4 = (bf16[16,2,128,128]{3,2,1,0:T(8,128)(2,1)}, bf16[16,2,128,128]{3,2,1,0:T(8,128)(2,1)S(1)}, u32[]{:S(2)}) copy-start(bf16[16,2,128,128]{3,2,1,0:T(8,128)(2,1)S(1)} %all-to-all-done.2) | copy-start | bytes 3145732
  70.6 31.5 %all-to-all-start.1 = ((bf16[16,2,128,128]{3,2,1,0:T(8,128)(2,1)}), bf16[16,2,128,128]{3,2,1,0:T(8,128)(2,1)}, u32[]{:S(2)}, u32[]{:S(2)}) async-start(bf16[16,2,128,128]{3,2,1,0:T(8,128)(2,1)} %bitcast.8), calls=%async_computation.1 | async-start | bytes 2097152 | tf_op jit(solution)/shard_map/all_to_all | solution.py:102
  75.1 2.6 %copy-start.10 = (bf16[2048,192]{0,1:T(8,128)(2,1)S(1)}, bf16[2048,192]{0,1:T(8,128)(2,1)}, u32[]{:S(2)}) copy-start(bf16[2048,192]{0,1:T(8,128)(2,1)} %param.21) | copy-start | bytes 2359300
  107.0 2.0 %copy-start.5 = (bf16[128,2048]{1,0:T(8,128)(2,1)S(1)}, bf16[128,2048]{1,0:T(8,128)(2,1)}, u32[]{:S(2)}) copy-start(bf16[128,2048]{1,0:T(8,128)(2,1)} %param.29) | copy-start | bytes 1572868
where the time goes:
time: 141 us
  waiting for transfers between devices  37.3 us (26%)
  starting transfers between devices  35.6 us (25%)
  blocking collectives  30.6 us (22%)
  matrix products  18.3 us (13%)
  local copies, waits for them, and re-layouts  12.8 us (9%)
  other arithmetic  5.97 us (4%)
    all_to_all x1, blocking collectives, summed_on_arrival(): lax.all_to_all(parts, axis, split_axis=0, concat_axis=0, tiled=True)  30.6 us
    all_to_all x1, starting transfers between devices, local(): lax.all_to_all(table, 'st', split_axis=0, concat_axis=0, tiled=True)  23.7 us
    all_to_all x1, waiting for transfers between devices, local(): lax.all_to_all(key_store[wanted], 'st', split_axis=0, concat_axis=0, tile...  20.7 us
    all_to_all x1, waiting for transfers between devices, local(): lax.all_to_all(value_store[wanted], 'st', split_axis=0, concat_axis=0, ti...  16.7 us
    all_to_all x1, starting transfers between devices, local(): lax.all_to_all(key_store[wanted], 'st', split_axis=0, concat_axis=0, tile...  7.5 us
    all_to_all x1, starting transfers between devices, local(): lax.all_to_all(value_store[wanted], 'st', split_axis=0, concat_axis=0, ti...  4.44 us
    reduce_sum x2, other arithmetic, row_norm(): jnp.mean(widened * widened, axis=-1, keepdims=True) + eps  3.51 us
    dot_general x1, matrix products, local(): jnp.dot(held_rows, w_value, preferred_element_type=jnp.float32)  3.44 us
  transfers between devices with their start and end apart: 3, of which 2 were waited for; matrix products, arithmetic and copies ran while one was open for 16% of the time, Pallas kernels for 0%

commit v1 on v0

v1 whole, which is shorter than its diff:
```python
import functools

import jax
import jax.numpy as jnp
from jax import lax
from jax.experimental import pallas as pl
from jax.experimental.pallas import tpu as pltpu
from jax.sharding import PartitionSpec as P

HD = 128
SPAN = 128
RBLOCK = 64
NPB = 4
PROWS = 128
NORM_ROWS = 32
PIECES = 4

MESH = pl.DeviceIdType.MESH
eps = 1e-06
F32 = jnp.float32
BF16 = jnp.bfloat16


def dot(a, b, dims=((1,), (0,))):
    return lax.dot_general(a, b, (dims, ((), ())), preferred_element_type=F32)


def row_norm(source, gain, target, rows):
    def some(i, carry):
        at = pl.ds(pl.multiple_of(i * NORM_ROWS, NORM_ROWS), NORM_ROWS)
        wide = source[at, :].astype(F32)
        scale = lax.rsqrt(jnp.mean(wide * wide, axis=-1, keepdims=True) + eps)
        target[at, :] = (wide * scale * gain).astype(BF16)
        return carry

    lax.fori_loop(0, rows // NORM_ROWS, some, 0)


def kernel(
    n_st,
    n_tp,
    tokens,
    pre_gain,
    w_gated,
    w_mixed,
    mix_weight,
    w_query,
    w_gate_mix,
    w_gate_read,
    store,
    mem_gain,
    w_key,
    w_value,
    ids,
    w_out_mix,
    w_out_read,
    out,
    tok,
    normed,
    wg,
    wm,
    wgm,
    mixw,
    wq,
    wgr,
    wkv,
    wom,
    wor,
    rows_in,
    rows_norm,
    key_of,
    value_of,
    q_ring,
    q_sib,
    ids_all,
    o_send,
    s_send,
    ret_o,
    ret_s,
    gate_t,
    out_mix,
    out_read,
    part,
    rs_send,
    rs_recv,
    in_sem,
    row_sem,
    ids_send_sem,
    ids_recv_sem,
    ring_send_sem,
    ring_recv_sem,
    sib_send_sem,
    sib_recv_sem,
    ret_send_sem,
    ret_recv_sem,
    stat_send_sem,
    stat_recv_sem,
    rs_send_sem,
    rs_recv_sem,
):
    grp, st, tp = lax.axis_index("grp"), lax.axis_index("st"), lax.axis_index("tp")
    n_y = n_st // 2
    half_y, half_tp = n_y // 2, n_tp // 2
    y, core = st // 2, lax.rem(st, 2)
    count = tok.shape[0]
    blocks = count // RBLOCK
    per_owner = rows_in.shape[0]
    mine_rows = count // n_tp

    def at_y(offset, sibling=False):
        chip = lax.rem(y + offset + n_y, n_y)
        return chip * 2 + (1 - core if sibling else core)

    def along_tp(offset):
        return lax.rem(tp + offset + n_tp, n_tp)

    barrier = pltpu.get_barrier_semaphore()
    peers = [(grp, lax.rem(st + k, n_st), tp) for k in range(1, n_st)]
    sides = [1, -1] if n_tp > 2 else [1]
    peers += [(grp, st, along_tp(k)) for k in sides]
    for peer in peers:
        pl.semaphore_signal(barrier, inc=1, device_id=peer, device_id_type=MESH)

    def fetch(k, source, target):
        copy = pltpu.make_async_copy(source, target, in_sem.at[k])
        copy.start()
        return copy

    got_tok = fetch(0, tokens, tok)
    got_wq = fetch(1, w_query, wq)
    got_wk = fetch(2, w_key, wkv.at[:, 0:HD])
    got_wv = fetch(3, w_value, wkv.at[:, HD : 2 * HD])
    got_rows = []
    for p in range(per_owner):
        copy = pltpu.make_async_copy(store.at[p], rows_in.at[p], row_sem.at[p])
        copy.start()
        got_rows.append(copy)
    got_wm = fetch(4, w_mixed, wm)
    got_wg = fetch(5, w_gated, wg)
    got_wgm = fetch(6, w_gate_mix, wgm)
    got_wgr = fetch(7, w_gate_read, wgr)
    got_mixw = fetch(8, mix_weight.at[0], mixw)
    got_wom = fetch(9, w_out_mix, wom)
    got_wor = fetch(10, w_out_read, wor)

    got_tok.wait()
    row_norm(tok, pre_gain[...].reshape(1, -1), normed, count)
    got_wq.wait()
    own_q = dot(normed[...], wq[...]).astype(BF16)
    q_ring[0][...] = own_q.reshape(blocks, RBLOCK, HD)

    pl.semaphore_wait(barrier, len(peers))

    id_copies = []
    for k in range(1, n_st):
        copy = pltpu.make_async_remote_copy(
            ids, ids_all.at[st], ids_send_sem.at[k], ids_recv_sem.at[k],
            device_id=(grp, lax.rem(st + k, n_st), tp), device_id_type=MESH,
        )
        copy.start()
        id_copies.append(copy)
    for b in range(blocks):
        for n in range(NPB):
            ids_all[st, b, n] = ids[b, n]

    cut = blocks // 2
    ring_copies, sib_copies = {}, {}

    def push(j, h, up):
        after = j + 1 if up else (j - 1) % n_y
        piece = pl.ds(h * cut, cut)
        copy = pltpu.make_async_remote_copy(
            q_ring[j].at[piece], q_ring[after].at[piece],
            ring_send_sem.at[after, h], ring_recv_sem.at[after, h],
            device_id=(grp, at_y(1 if up else -1), tp), device_id_type=MESH,
        )
        copy.start()
        ring_copies[after, h] = copy

    def across(j, h):
        piece = pl.ds(h * cut, cut)
        copy = pltpu.make_async_remote_copy(
            q_ring[j].at[piece], q_sib[j].at[piece],
            sib_send_sem.at[j, h], sib_recv_sem.at[j, h],
            device_id=(grp, at_y(0, True), tp), device_id_type=MESH,
        )
        copy.start()
        sib_copies[j, h] = copy

    def onward(j, h):
        if j < half_y and (j + 1 < half_y or h == 0):
            push(j, h, True)
        if (j == 0 or j > half_y) and (n_y - 1 if j == 0 else j - 1) >= half_y:
            if (n_y - 1 if j == 0 else j - 1) > half_y or h == 1:
                push(j, h, False)

    def arrive(k):
        for h in range(2):
            for j in sorted({k, n_y - k}):
                if k == half_y or True:
                    ring_copies[j, h].wait_recv()
                    if j != half_y:
                        onward(j, h)
                    across(j, h)

    for h in range(2):
        onward(0, h)
    for h in range(2):
        across(0, h)

    got_wk.wait()
    got_wv.wait()
    mem_row = mem_gain[...].reshape(1, -1)

    def keys_of(low, high):
        def one(p, carry):
            pltpu.make_async_copy(store.at[p], rows_in.at[p], row_sem.at[p]).wait()
            row_norm(rows_in.at[p], mem_row, rows_norm, PROWS)
            both = dot(rows_norm[...], wkv[...])
            key_of[p] = both[:, :HD].astype(BF16)
            value_of[p] = jnp.transpose(both[:, HD:]).astype(BF16)
            return carry

        lax.fori_loop(low, high, one, 0)

    lanes = lax.broadcasted_iota(jnp.int32, (1, 2 * RBLOCK), 1)
    first_half = lanes < RBLOCK

    def slots_of(reader):
        p0 = p1 = b0 = b1 = seen = jnp.int32(0)
        for b in range(blocks):
            for n in range(NPB):
                local = ids_all[reader, b, n] - st * per_owner
                mine = (local >= 0) & (local < per_owner)
                is0 = mine & (seen == 0)
                is1 = mine & (seen == 1)
                p0, b0 = jnp.where(is0, local, p0), jnp.where(is0, b, b0)
                p1, b1 = jnp.where(is1, local, p1), jnp.where(is1, b, b1)
                seen = seen + jnp.where(mine, 1, 0)
        return p0, p1, b0, b1

    def attend(q_ref, reader):
        p0, p1, b0, b1 = slots_of(reader)
        q = jnp.concatenate([q_ref[b0], q_ref[b1]], axis=0)
        over_keys = ((1,), (1,))
        scores = jnp.where(
            first_half, dot(key_of[p0], q, over_keys), dot(key_of[p1], q, over_keys)
        ) * (HD ** (-0.5))
        top = jnp.max(scores, axis=0, keepdims=True)
        weight = jnp.exp(scores - top)
        total = jnp.sum(weight, axis=0, keepdims=True)
        weight = weight.astype(BF16)
        read = jnp.where(first_half, dot(value_of[p0], weight), dot(value_of[p1], weight))
        return read.astype(BF16), jnp.concatenate([top, total], axis=0)

    ret_copies = []

    def serve(j, sibling):
        reader = at_y(-j, sibling)
        read, stats = attend(q_sib[j] if sibling else q_ring[j], reader)
        if j == 0 and not sibling:
            ret_o[st] = read
            ret_s[st] = stats
            return
        label = j * 2 + (1 if sibling else 0)
        o_send[label] = read
        s_send[label] = stats
        for source, target, send, recv in (
            (o_send, ret_o, ret_send_sem, ret_recv_sem),
            (s_send, ret_s, stat_send_sem, stat_recv_sem),
        ):
            copy = pltpu.make_async_remote_copy(
                source.at[label], target.at[st], send.at[label], recv.at[label],
                device_id=(grp, reader, tp), device_id_type=MESH,
            )
            copy.start()
            ret_copies.append(copy)

    def serve_pair(j):
        serve(j, False)
        for h in range(2):
            sib_copies[j, h].wait_recv()
        serve(j, True)

    half_owner = per_owner // 2
    keys_of(0, half_owner)
    if half_y > 1:
        arrive(1)
    keys_of(half_owner, per_owner)
    for copy in id_copies:
        copy.wait_recv()
    for k in range(1, half_y + 1):
        if k > 1 or half_y == 1:
            arrive(k)
        if k == 1:
            serve_pair(0)
        else:
            for j in sorted({k - 1, n_y - k + 1}):
                serve_pair(j)
    serve_pair(half_y)

    got_wm.wait()
    mixed_in = dot(normed[...], wm[...])
    centred = mixed_in - jnp.mean(mixed_in, axis=-1, keepdims=True)
    variance = jnp.mean(centred * centred, axis=-1, keepdims=True)
    mixed_norm = (centred * lax.rsqrt(variance + eps)).astype(BF16)
    got_mixw.wait()
    row_at = lax.broadcasted_iota(jnp.int32, (SPAN, SPAN), 0)
    col_at = lax.broadcasted_iota(jnp.int32, (SPAN, SPAN), 1)
    causal = jnp.where(col_at <= row_at, mixw[...].astype(F32), 0.0).astype(BF16)
    spatial = jnp.concatenate(
        [dot(causal, mixed_norm[n * SPAN : (n + 1) * SPAN]) for n in range(count // SPAN)], axis=0
    )
    got_wg.wait()
    branch_mix = dot(normed[...], wg[...]) * spatial
    got_wgm.wait()
    gate = dot(normed[...], wgm[...])
    out_mix[...] = (branch_mix * (gate / (1.0 + jnp.exp(-gate)))).astype(BF16)
    got_wgr.wait()
    gate = dot(normed[...], wgr[...])
    gate_t[...] = jnp.transpose(gate / (1.0 + jnp.exp(-gate)))
    got_wom.wait()
    width = part.shape[2]
    for c in range(PIECES):
        part[c] = dot(out_mix[...], wom[:, c * width : (c + 1) * width])

    owners, ranks = [], []
    for e in range(blocks * NPB):
        owner = ids[e // NPB, e % NPB] // per_owner
        rank = jnp.int32(0)
        for before in owners:
            rank = rank + jnp.where(before == owner, 1, 0)
        owners.append(owner)
        ranks.append(rank)
    for copy in ret_copies:
        copy.wait_recv()
    got_wor.wait()
    for pair in range(blocks // 2):
        tops, totals, reads = [], [], []
        for n in range(NPB):
            e0, e1 = pair * 2 * NPB + n, (pair * 2 + 1) * NPB + n

            def placed(ref):
                x0, x1 = ref[owners[e0]].astype(F32), ref[owners[e1]].astype(F32)
                low = jnp.where(ranks[e0] == 0, x0, pltpu.roll(x0, RBLOCK, 1))
                high = jnp.where(ranks[e1] == 1, x1, pltpu.roll(x1, RBLOCK, 1))
                return jnp.where(first_half, low, high)

            stats = placed(ret_s)
            tops.append(stats[0:1])
            totals.append(stats[1:2])
            reads.append(placed(ret_o))
        top = functools.reduce(jnp.maximum, tops)
        scales = [jnp.exp(t - top) for t in tops]
        total = sum(s * t for s, t in zip(scales, totals))
        read = sum(s * r for s, r in zip(scales, reads)) / total
        cols = slice(pair * 2 * RBLOCK, (pair + 1) * 2 * RBLOCK)
        out_read[cols, :] = jnp.transpose(read * gate_t[:, cols]).astype(BF16)

    rs_copies = {}

    def pass_on(c, d, k):
        sign = 1 - 2 * d
        target = along_tp(sign * k)
        lo = 0
        size = mine_rows
        if k == half_tp:
            size = mine_rows // 2
            lo = d * size
        start = pl.multiple_of(target * mine_rows + lo, mine_rows // 2)
        value = part[c, pl.ds(start, size), :]
        if k == half_tp:
            rs_send[d, k - 1, c, lo : lo + size, :] = value.astype(BF16)
        else:
            rs_copies[c, d, k + 1].wait_recv()
            if k + 1 == half_tp:
                cut_rows = mine_rows // 2
                low = d * cut_rows
                rs_send[d, k - 1, c, low : low + cut_rows, :] = (
                    part[c, pl.ds(pl.multiple_of(target * mine_rows + low, cut_rows), cut_rows), :]
                    + rs_recv[d, k, c, low : low + cut_rows, :].astype(F32)
                ).astype(BF16)
                other = cut_rows - low
                rs_send[d, k - 1, c, other : other + cut_rows, :] = part[
                    c, pl.ds(pl.multiple_of(target * mine_rows + other, cut_rows), cut_rows), :
                ].astype(BF16)
            else:
                rs_send[d, k - 1, c] = (value + rs_recv[d, k, c].astype(F32)).astype(BF16)
        copy = pltpu.make_async_remote_copy(
            rs_send.at[d, k - 1, c, pl.ds(lo, size)], rs_recv.at[d, k - 1, c, pl.ds(lo, size)],
            rs_send_sem.at[d, k - 1, c], rs_recv_sem.at[d, k - 1, c],
            device_id=(grp, st, along_tp(sign)), device_id_type=MESH,
        )
        copy.start()
        rs_copies[c, d, k] = copy

    for c in range(PIECES):
        part[c] = part[c] + dot(out_read[...], wor[:, c * width : (c + 1) * width])
        for d in range(2):
            pass_on(c, d, half_tp)
    for k in range(half_tp - 1, 0, -1):
        for c in range(PIECES):
            for d in range(2):
                pass_on(c, d, k)
    here = pl.ds(pl.multiple_of(tp * mine_rows, mine_rows), mine_rows)
    for c in range(PIECES):
        for d in range(2):
            rs_copies[c, d, 1].wait_recv()
        if half_tp == 1:
            cut_rows = mine_rows // 2
            both = jnp.concatenate(
                [rs_recv[0, 0, c, :cut_rows, :], rs_recv[1, 0, c, cut_rows:, :]], axis=0
            ).astype(F32)
        else:
            both = rs_recv[0, 0, c].astype(F32) + rs_recv[1, 0, c].astype(F32)
        out[:, c * width : (c + 1) * width] = (part[c, here, :] + both).astype(BF16)

    for copy in (
        id_copies + list(ring_copies.values()) + list(sib_copies.values())
        + ret_copies + list(rs_copies.values())
    ):
        copy.wait_send()


def local(*args, n_st, n_tp):
    tokens, w_gated, store = args[0], args[2], args[8]
    count, width = tokens.shape
    mix_width = w_gated.shape[1]
    held = store.shape[0]
    blocks = count // RBLOCK
    n_y = n_st // 2
    mine_rows = count // n_tp
    hbm = pl.BlockSpec(memory_space=pltpu.HBM)
    vmem = pl.BlockSpec(memory_space=pltpu.VMEM)
    smem = pl.BlockSpec(memory_space=pltpu.SMEM)
    specs = [hbm] * 15
    specs[1] = specs[9] = vmem
    specs[12] = smem
    dma = pltpu.SemaphoreType.DMA
    columns = width // PIECES
    scratch = dict(
        tok=pltpu.VMEM((count, width), BF16),
        normed=pltpu.VMEM((count, width), BF16),
        wg=pltpu.VMEM((width, mix_width), BF16),
        wm=pltpu.VMEM((width, mix_width), BF16),
        wgm=pltpu.VMEM((width, mix_width), BF16),
        mixw=pltpu.VMEM((SPAN, SPAN), BF16),
        wq=pltpu.VMEM((width, HD), BF16),
        wgr=pltpu.VMEM((width, HD), BF16),
        wkv=pltpu.VMEM((width, 2 * HD), BF16),
        wom=pltpu.VMEM((mix_width, width), BF16),
        wor=pltpu.VMEM((HD, width), BF16),
        rows_in=pltpu.VMEM((held, PROWS, width), BF16),
        rows_norm=pltpu.VMEM((PROWS, width), BF16),
        key_of=pltpu.VMEM((held, PROWS, HD), BF16),
        value_of=pltpu.VMEM((held, HD, PROWS), BF16),
        q_ring=[pltpu.VMEM((blocks, RBLOCK, HD), BF16) for _ in range(n_y)],
        q_sib=[pltpu.VMEM((blocks, RBLOCK, HD), BF16) for _ in range(n_y)],
        ids_all=pltpu.SMEM((n_st, blocks, NPB), jnp.int32),
        o_send=pltpu.VMEM((n_st, HD, 2 * RBLOCK), BF16),
        s_send=pltpu.VMEM((n_st, 2, 2 * RBLOCK), F32),
        ret_o=pltpu.VMEM((n_st, HD, 2 * RBLOCK), BF16),
        ret_s=pltpu.VMEM((n_st, 2, 2 * RBLOCK), F32),
        gate_t=pltpu.VMEM((HD, count), F32),
        out_mix=pltpu.VMEM((count, mix_width), BF16),
        out_read=pltpu.VMEM((count, HD), BF16),
        part=pltpu.VMEM((PIECES, count, columns), F32),
        rs_send=pltpu.VMEM((2, n_tp // 2, PIECES, mine_rows, columns), BF16),
        rs_recv=pltpu.VMEM((2, n_tp // 2, PIECES, mine_rows, columns), BF16),
        in_sem=dma((11,)),
        row_sem=dma((held,)),
        ids_send_sem=dma((n_st,)),
        ids_recv_sem=dma((n_st,)),
        ring_send_sem=dma((n_y, 2)),
        ring_recv_sem=dma((n_y, 2)),
        sib_send_sem=dma((n_y, 2)),
        sib_recv_sem=dma((n_y, 2)),
        ret_send_sem=dma((n_st,)),
        ret_recv_sem=dma((n_st,)),
        stat_send_sem=dma((n_st,)),
        stat_recv_sem=dma((n_st,)),
        rs_send_sem=dma((2, n_tp // 2, PIECES)),
        rs_recv_sem=dma((2, n_tp // 2, PIECES)),
    )
    names = list(scratch)

    def body(*refs):
        kernel(n_st, n_tp, *refs[:16], **dict(zip(names, refs[16:])))

    return pl.pallas_call(
        body,
        out_shape=jax.ShapeDtypeStruct((mine_rows, width), BF16),
        in_specs=specs,
        out_specs=vmem,
        scratch_shapes=list(scratch.values()),
        compiler_params=pltpu.CompilerParams(
            collective_id=0, has_side_effects=True, vmem_limit_bytes=48 * 1024 * 1024
        ),
        name="layer",
    )(*args)


def solution(mesh):
    placed = (
        P(("grp", "st"), None),
        P(),
        P(None, "tp"),
        P(None, "tp"),
        P("tp", None, None),
        P(None, "tp"),
        P(None, "tp"),
        P(None, "tp"),
        P(("grp", "st"), None, None),
        P(),
        P(None, "tp"),
        P(None, "tp"),
        P(("grp", "st"), None),
        P("tp", None),
        P("tp", None),
    )
    body = functools.partial(local, n_st=mesh.shape["st"], n_tp=mesh.shape["tp"])
    return jax.shard_map(
        body, mesh=mesh, in_specs=placed, out_specs=P(("grp", "st", "tp"), None), check_vma=False
    )
```

time: 141 us -> 78.5 us (0.56)
  the two profiles are of different devices: /device:TPU:513 before, /device:TPU:514 now
where the time goes in v1:
time: 78.5 us; the launch traced here: 78.2 us
  Pallas kernels  67.2 us (86%)
  local copies, waits for them, and re-layouts  10.9 us (14%)
    pallas_call x1, Pallas kernels, local(): pl.pallas_call(body, out_shape=jax.ShapeDtypeStruct((mine_rows, width), B...  67.2 us
    unnamed x26, local copies, waits for them, and re-layouts  10.9 us

profile of v1, /device:TPU:514, one launch (start us, length us, event | category | flops | bytes accessed | tf_op | source)
XLA Modules:
  0.0 78.2 jit_solution(322049081948310257)
XLA Ops:
  0.0 0.0 copy-start.1
  0.0 0.0 copy-start.10
  0.0 0.0 copy-start.9
  0.0 0.0 copy-start.2
  0.0 0.0 copy-start.7
  0.0 0.0 copy-start.8
  0.0 0.0 copy-start
  0.0 1.6 %copy.16.refs_2_ = bf16[2048,192]{1,0:T(8,128)(2,1)S(1)} copy(bf16[2048,192]{0,1:T(8,128)(2,1)} %param.17) | data formatting | bytes 1572864 | tf_op args[2]
  1.6 2.2 %copy.17.refs_3_ = bf16[2048,192]{1,0:T(8,128)(2,1)} copy(bf16[2048,192]{0,1:T(8,128)(2,1)} %param.18) | data formatting | bytes 1572864 | tf_op args[3]
  3.9 2.2 %copy.18.refs_6_ = bf16[2048,192]{1,0:T(8,128)(2,1)} copy(bf16[2048,192]{0,1:T(8,128)(2,1)} %param.21) | data formatting | bytes 1572864 | tf_op args[6]
  6.1 0.0 copy-done.1
  6.1 0.0 copy-done.10
  6.1 0.0 copy-done.9
  6.1 0.0 copy-done.2
  6.1 0.0 copy-done.7
  6.1 0.0 copy-done.8
  6.1 0.0 copy-done
  6.1 0.0 copy-start.3
  6.1 1.0 %copy-done.3 = bf16[2048,128]{1,0:T(8,128)(2,1)S(1)} copy-done((bf16[2048,128]{1,0:T(8,128)(2,1)S(1)}, bf16[2048,128]{1,0:T(8,128)(2,1)}, u32[]{:S(2)}) %copy-start.3) | copy-done | bytes 524312
  7.2 0.0 copy-start.4
  7.2 1.0 %copy-done.4 = bf16[2048,128]{1,0:T(8,128)(2,1)S(1)} copy-done((bf16[2048,128]{1,0:T(8,128)(2,1)S(1)}, bf16[2048,128]{1,0:T(8,128)(2,1)}, u32[]{:S(2)}) %copy-start.4) | copy-done | bytes 524312
  8.2 0.0 copy-start.5
  8.2 1.0 %copy-done.5 = bf16[2048,128]{1,0:T(8,128)(2,1)S(1)} copy-done((bf16[2048,128]{1,0:T(8,128)(2,1)S(1)}, bf16[2048,128]{1,0:T(8,128)(2,1)}, u32[]{:S(2)}) %copy-start.5) | copy-done | bytes 524312
  9.3 0.0 copy-start.6
  9.3 1.0 %copy-done.6 = bf16[128,2048]{1,0:T(8,128)(2,1)S(1)} copy-done((bf16[128,2048]{1,0:T(8,128)(2,1)S(1)}, bf16[128,2048]{1,0:T(8,128)(2,1)}, u32[]{:S(2)}) %copy-start.6) | copy-done | bytes 524312
  10.3 67.2 %layer.1 = bf16[32,2048]{1,0:T(8,128)(2,1)S(1)} custom-call(bf16[256,2048]{1,0:T(8,128)(2,1)S(1)} %copy-done, f32[2048]{0:T(1024)S(1)} %copy-done.8, bf16[2048,192]{1,0:T(8,128)(2,1)S(1)} %copy.16.refs_2_, bf16[2048,192]{1,0:T(8,128)(2,1)} %copy.17.refs_3_, bf16[1,128,128]{2,1,0:T(8,128)(2,1)S(1)} %copy-done.7, bf16[2048,128]{1,0:T(8,128)(2,1)S(1)} %copy-done.2, ...), custom_call_target="tpu_custom_call" | custom-call | tf_op jit(solution)/shard_map/layer/pallas_call | solution.py:490
  77.5 0.7 copy.20
Async XLA Ops:
  0.0 6.1 %copy-start.1 = (bf16[192,2048]{1,0:T(8,128)(2,1)S(1)}, bf16[192,2048]{1,0:T(8,128)(2,1)}, u32[]{:S(2)}) copy-start(bf16[192,2048]{1,0:T(8,128)(2,1)} %refs_13_.1) | copy-start | bytes 2359300
  0.0 6.1 %copy-start.10 = (s32[4,4]{1,0:T(4,128)S(1)}, s32[4,4]{1,0:T(4,128)}, u32[]{:S(2)}) copy-start(s32[4,4]{1,0:T(4,128)} %refs_12_.1) | copy-start | bytes 196
  0.0 6.1 %copy-start.9 = (f32[2048]{0:T(1024)S(1)}, f32[2048]{0:T(1024)}, u32[]{:S(2)}) copy-start(f32[2048]{0:T(1024)} %refs_9_.1) | copy-start | bytes 24580
  0.0 6.1 %copy-start.2 = (bf16[2048,128]{1,0:T(8,128)(2,1)S(1)}, bf16[2048,128]{1,0:T(8,128)(2,1)}, u32[]{:S(2)}) copy-start(bf16[2048,128]{1,0:T(8,128)(2,1)} %refs_5_.1) | copy-start | bytes 1572868
  0.0 6.1 %copy-start.7 = (bf16[1,128,128]{2,1,0:T(8,128)(2,1)S(1)}, bf16[1,128,128]{2,1,0:T(8,128)(2,1)}, u32[]{:S(2)}) copy-start(bf16[1,128,128]{2,1,0:T(8,128)(2,1)} %refs_4_.1) | copy-start | bytes 98308
  0.0 6.1 %copy-start.8 = (f32[2048]{0:T(1024)S(1)}, f32[2048]{0:T(1024)}, u32[]{:S(2)}) copy-start(f32[2048]{0:T(1024)} %refs_1_.1) | copy-start | bytes 24580
  0.0 6.1 %copy-start = (bf16[256,2048]{1,0:T(8,128)(2,1)S(1)}, bf16[256,2048]{1,0:T(8,128)(2,1)}, u32[]{:S(2)}) copy-start(bf16[256,2048]{1,0:T(8,128)(2,1)} %refs_0_.1) | copy-start | bytes 3145732
  6.1 1.0 %copy-start.3 = (bf16[2048,128]{1,0:T(8,128)(2,1)S(1)}, bf16[2048,128]{1,0:T(8,128)(2,1)}, u32[]{:S(2)}) copy-start(bf16[2048,128]{1,0:T(8,128)(2,1)} %refs_7_.1) | copy-start | bytes 1572868
  7.2 1.0 %copy-start.4 = (bf16[2048,128]{1,0:T(8,128)(2,1)S(1)}, bf16[2048,128]{1,0:T(8,128)(2,1)}, u32[]{:S(2)}) copy-start(bf16[2048,128]{1,0:T(8,128)(2,1)} %refs_10_.1) | copy-start | bytes 1572868
  8.2 1.0 %copy-start.5 = (bf16[2048,128]{1,0:T(8,128)(2,1)S(1)}, bf16[2048,128]{1,0:T(8,128)(2,1)}, u32[]{:S(2)}) copy-start(bf16[2048,128]{1,0:T(8,128)(2,1)} %refs_11_.1) | copy-start | bytes 1572868
  9.3 1.0 %copy-start.6 = (bf16[128,2048]{1,0:T(8,128)(2,1)S(1)}, bf16[128,2048]{1,0:T(8,128)(2,1)}, u32[]{:S(2)}) copy-start(bf16[128,2048]{1,0:T(8,128)(2,1)} %refs_14_.1) | copy-start | bytes 1572868

commit v2 on v1

--- a/solution.py
+++ b/solution.py
@@ -197,11 +197,10 @@
     def arrive(k):
         for h in range(2):
             for j in sorted({k, n_y - k}):
-                if k == half_y or True:
-                    ring_copies[j, h].wait_recv()
-                    if j != half_y:
-                        onward(j, h)
-                    across(j, h)
+                ring_copies[j, h].wait_recv()
+                if j != half_y:
+                    onward(j, h)
+                across(j, h)
 
     for h in range(2):
         onward(0, h)
@@ -300,7 +299,8 @@
     serve_pair(half_y)
 
     got_wm.wait()
-    mixed_in = dot(normed[...], wm[...])
+    over_width = ((1,), (1,))
+    mixed_in = dot(normed[...], wm[...], over_width)
     centred = mixed_in - jnp.mean(mixed_in, axis=-1, keepdims=True)
     variance = jnp.mean(centred * centred, axis=-1, keepdims=True)
     mixed_norm = (centred * lax.rsqrt(variance + eps)).astype(BF16)
@@ -312,9 +312,9 @@
         [dot(causal, mixed_norm[n * SPAN : (n + 1) * SPAN]) for n in range(count // SPAN)], axis=0
     )
     got_wg.wait()
-    branch_mix = dot(normed[...], wg[...]) * spatial
+    branch_mix = dot(normed[...], wg[...], over_width) * spatial
     got_wgm.wait()
-    gate = dot(normed[...], wgm[...])
+    gate = dot(normed[...], wgm[...], over_width)
     out_mix[...] = (branch_mix * (gate / (1.0 + jnp.exp(-gate)))).astype(BF16)
     got_wgr.wait()
     gate = dot(normed[...], wgr[...])
@@ -423,9 +423,10 @@
 
 
 def local(*args, n_st, n_tp):
+    args = [a.T if k in (2, 3, 6) else a for k, a in enumerate(args)]
     tokens, w_gated, store = args[0], args[2], args[8]
     count, width = tokens.shape
-    mix_width = w_gated.shape[1]
+    mix_width = w_gated.shape[0]
     held = store.shape[0]
     blocks = count // RBLOCK
     n_y = n_st // 2
@@ -441,9 +442,9 @@
     scratch = dict(
         tok=pltpu.VMEM((count, width), BF16),
         normed=pltpu.VMEM((count, width), BF16),
-        wg=pltpu.VMEM((width, mix_width), BF16),
-        wm=pltpu.VMEM((width, mix_width), BF16),
-        wgm=pltpu.VMEM((width, mix_width), BF16),
+        wg=pltpu.VMEM((mix_width, width), BF16),
+        wm=pltpu.VMEM((mix_width, width), BF16),
+        wgm=pltpu.VMEM((mix_width, width), BF16),
         mixw=pltpu.VMEM((SPAN, SPAN), BF16),
         wq=pltpu.VMEM((width, HD), BF16),
         wgr=pltpu.VMEM((width, HD), BF16),
@@ -494,7 +495,7 @@
         out_specs=vmem,
         scratch_shapes=list(scratch.values()),
         compiler_params=pltpu.CompilerParams(
-            collective_id=0, has_side_effects=True, vmem_limit_bytes=48 * 1024 * 1024
+            collective_id=0, has_side_effects=True, vmem_limit_bytes=67_000_000
         ),
         name="layer",
     )(*args)

time: 78.5 us -> 69.5 us (0.89)
  the two profiles are of different devices: /device:TPU:514 before, /device:TPU:513 now
where the time goes in v2:
time: 69.5 us; the launch traced here: 69.3 us
  Pallas kernels  67.7 us (97%)
  local copies, waits for them, and re-layouts  1.57 us (2%)
    pallas_call x1, Pallas kernels, local(): pl.pallas_call(body, out_shape=jax.ShapeDtypeStruct((mine_rows, width), B...  67.7 us
    unnamed x1, local copies, waits for them, and re-layouts  1.57 us

profile of v2, /device:TPU:513, one launch (start us, length us, event | category | flops | bytes accessed | tf_op | source)
XLA Modules:
  0.0 69.3 jit_solution(11913895479289037356)
XLA Ops:
  0.0 67.7 %layer.1 = bf16[32,2048]{1,0:T(8,128)(2,1)} custom-call(bf16[256,2048]{1,0:T(8,128)(2,1)} %refs_0_.1, f32[2048]{0:T(1024)} %refs_1_.1, bf16[192,2048]{1,0:T(8,128)(2,1)} %bitcast.3, bf16[192,2048]{1,0:T(8,128)(2,1)} %bitcast.4, bf16[1,128,128]{2,1,0:T(8,128)(2,1)} %refs_4_.1, bf16[2048,128]{1,0:T(8,128)(2,1)} %refs_5_.1, bf16[192,2048]{1,0:T(8,128)(2,1)} %bitcast.5, ...), custom_call_target="tpu_custom_call" | custom-call | tf_op jit(solution)/shard_map/layer/pallas_call | solution.py:491
  67.8 1.6 %copy.17 = bf16[32,2048]{1,0:T(8,128)(2,1)} copy(bf16[32,2048]{1,0:T(8,128)(2,1)} %layer.1) | data formatting | bytes 262144

commit v3 on v2

--- a/solution.py
+++ b/solution.py
@@ -56,6 +56,9 @@
     w_out_read,
     out,
     tok,
+    gains,
+    own_ids,
+    slot_of,
     normed,
     wg,
     wm,
@@ -100,7 +103,7 @@
 ):
     grp, st, tp = lax.axis_index("grp"), lax.axis_index("st"), lax.axis_index("tp")
     n_y = n_st // 2
-    half_y, half_tp = n_y // 2, n_tp // 2
+    half_tp = n_tp // 2
     y, core = st // 2, lax.rem(st, 2)
     count = tok.shape[0]
     blocks = count // RBLOCK
@@ -113,6 +116,16 @@
 
     def along_tp(offset):
         return lax.rem(tp + offset + n_tp, n_tp)
+
+    def fetch(k, source, target):
+        copy = pltpu.make_async_copy(source, target, in_sem.at[k])
+        copy.start()
+        return copy
+
+    got_tok = fetch(0, tokens, tok)
+    got_pre = fetch(11, pre_gain, gains.at[0])
+    got_wq = fetch(1, w_query, wq)
+    got_ids = fetch(12, ids, own_ids)
 
     barrier = pltpu.get_barrier_semaphore()
     peers = [(grp, lax.rem(st + k, n_st), tp) for k in range(1, n_st)]
@@ -121,20 +134,11 @@
     for peer in peers:
         pl.semaphore_signal(barrier, inc=1, device_id=peer, device_id_type=MESH)
 
-    def fetch(k, source, target):
-        copy = pltpu.make_async_copy(source, target, in_sem.at[k])
-        copy.start()
-        return copy
-
-    got_tok = fetch(0, tokens, tok)
-    got_wq = fetch(1, w_query, wq)
     got_wk = fetch(2, w_key, wkv.at[:, 0:HD])
     got_wv = fetch(3, w_value, wkv.at[:, HD : 2 * HD])
-    got_rows = []
+    got_mem = fetch(13, mem_gain, gains.at[1])
     for p in range(per_owner):
-        copy = pltpu.make_async_copy(store.at[p], rows_in.at[p], row_sem.at[p])
-        copy.start()
-        got_rows.append(copy)
+        pltpu.make_async_copy(store.at[p], rows_in.at[p], row_sem.at[p]).start()
     got_wm = fetch(4, w_mixed, wm)
     got_wg = fetch(5, w_gated, wg)
     got_wgm = fetch(6, w_gate_mix, wgm)
@@ -143,36 +147,25 @@
     got_wom = fetch(9, w_out_mix, wom)
     got_wor = fetch(10, w_out_read, wor)
 
+    got_pre.wait()
     got_tok.wait()
-    row_norm(tok, pre_gain[...].reshape(1, -1), normed, count)
+    row_norm(tok, gains[0].reshape(1, -1), normed, count)
     got_wq.wait()
     own_q = dot(normed[...], wq[...]).astype(BF16)
     q_ring[0][...] = own_q.reshape(blocks, RBLOCK, HD)
+    got_ids.wait()
 
     pl.semaphore_wait(barrier, len(peers))
-
-    id_copies = []
-    for k in range(1, n_st):
-        copy = pltpu.make_async_remote_copy(
-            ids, ids_all.at[st], ids_send_sem.at[k], ids_recv_sem.at[k],
-            device_id=(grp, lax.rem(st + k, n_st), tp), device_id_type=MESH,
-        )
-        copy.start()
-        id_copies.append(copy)
-    for b in range(blocks):
-        for n in range(NPB):
-            ids_all[st, b, n] = ids[b, n]
 
     cut = blocks // 2
     ring_copies, sib_copies = {}, {}
 
-    def push(j, h, up):
-        after = j + 1 if up else (j - 1) % n_y
+    def push(j, after, h, offset):
         piece = pl.ds(h * cut, cut)
         copy = pltpu.make_async_remote_copy(
             q_ring[j].at[piece], q_ring[after].at[piece],
             ring_send_sem.at[after, h], ring_recv_sem.at[after, h],
-            device_id=(grp, at_y(1 if up else -1), tp), device_id_type=MESH,
+            device_id=(grp, at_y(offset), tp), device_id_type=MESH,
         )
         copy.start()
         ring_copies[after, h] = copy
@@ -187,45 +180,46 @@
         copy.start()
         sib_copies[j, h] = copy
 
-    def onward(j, h):
-        if j < half_y and (j + 1 < half_y or h == 0):
-            push(j, h, True)
-        if (j == 0 or j > half_y) and (n_y - 1 if j == 0 else j - 1) >= half_y:
-            if (n_y - 1 if j == 0 else j - 1) > half_y or h == 1:
-                push(j, h, False)
-
-    def arrive(k):
-        for h in range(2):
-            for j in sorted({k, n_y - k}):
-                ring_copies[j, h].wait_recv()
-                if j != half_y:
-                    onward(j, h)
-                across(j, h)
-
-    for h in range(2):
-        onward(0, h)
+    for h in range(2):
+        push(0, 2, h, 2)
+        push(0, n_y - 2, h, -2)
+    for h in range(2):
+        push(0, 1, h, 1)
+        push(0, n_y - 1, h, -1)
     for h in range(2):
         across(0, h)
+
+    id_copies = []
+    for k in range(1, n_st):
+        copy = pltpu.make_async_remote_copy(
+            own_ids, ids_all.at[st], ids_send_sem.at[k], ids_recv_sem.at[k],
+            device_id=(grp, lax.rem(st + k, n_st), tp), device_id_type=MESH,
+        )
+        copy.start()
+        id_copies.append(copy)
+    for b in range(blocks):
+        for n in range(NPB):
+            ids_all[st, b, n] = own_ids[b, n]
 
     got_wk.wait()
     got_wv.wait()
-    mem_row = mem_gain[...].reshape(1, -1)
-
-    def keys_of(low, high):
-        def one(p, carry):
-            pltpu.make_async_copy(store.at[p], rows_in.at[p], row_sem.at[p]).wait()
-            row_norm(rows_in.at[p], mem_row, rows_norm, PROWS)
-            both = dot(rows_norm[...], wkv[...])
-            key_of[p] = both[:, :HD].astype(BF16)
-            value_of[p] = jnp.transpose(both[:, HD:]).astype(BF16)
-            return carry
-
-        lax.fori_loop(low, high, one, 0)
-
-    lanes = lax.broadcasted_iota(jnp.int32, (1, 2 * RBLOCK), 1)
-    first_half = lanes < RBLOCK
-
-    def slots_of(reader):
+    got_mem.wait()
+    mem_row = gains[1].reshape(1, -1)
+
+    def keys_of(p, carry):
+        pltpu.make_async_copy(store.at[p], rows_in.at[p], row_sem.at[p]).wait()
+        row_norm(rows_in.at[p], mem_row, rows_norm, PROWS)
+        both = dot(rows_norm[...], wkv[...])
+        key_of[p] = both[:, :HD].astype(BF16)
+        value_of[p] = jnp.transpose(both[:, HD:]).astype(BF16)
+        return carry
+
+    lax.fori_loop(0, per_owner, keys_of, 0)
+
+    for copy in id_copies:
+        copy.wait_recv()
+
+    def slots(reader, carry):
         p0 = p1 = b0 = b1 = seen = jnp.int32(0)
         for b in range(blocks):
             for n in range(NPB):
@@ -236,10 +230,17 @@
                 p0, b0 = jnp.where(is0, local, p0), jnp.where(is0, b, b0)
                 p1, b1 = jnp.where(is1, local, p1), jnp.where(is1, b, b1)
                 seen = seen + jnp.where(mine, 1, 0)
-        return p0, p1, b0, b1
+        for k, value in enumerate((p0, p1, b0, b1)):
+            slot_of[reader, k] = value
+        return carry
+
+    lax.fori_loop(0, n_st, slots, 0)
+
+    lanes = lax.broadcasted_iota(jnp.int32, (1, 2 * RBLOCK), 1)
+    first_half = lanes < RBLOCK
 
     def attend(q_ref, reader):
-        p0, p1, b0, b1 = slots_of(reader)
+        p0, p1, b0, b1 = (slot_of[reader, k] for k in range(4))
         q = jnp.concatenate([q_ref[b0], q_ref[b1]], axis=0)
         over_keys = ((1,), (1,))
         scores = jnp.where(
@@ -254,49 +255,54 @@
 
     ret_copies = []
 
-    def serve(j, sibling):
-        reader = at_y(-j, sibling)
-        read, stats = attend(q_sib[j] if sibling else q_ring[j], reader)
-        if j == 0 and not sibling:
-            ret_o[st] = read
-            ret_s[st] = stats
-            return
-        label = j * 2 + (1 if sibling else 0)
-        o_send[label] = read
-        s_send[label] = stats
-        for source, target, send, recv in (
-            (o_send, ret_o, ret_send_sem, ret_recv_sem),
-            (s_send, ret_s, stat_send_sem, stat_recv_sem),
-        ):
-            copy = pltpu.make_async_remote_copy(
-                source.at[label], target.at[st], send.at[label], recv.at[label],
-                device_id=(grp, reader, tp), device_id_type=MESH,
-            )
-            copy.start()
-            ret_copies.append(copy)
-
-    def serve_pair(j):
-        serve(j, False)
-        for h in range(2):
-            sib_copies[j, h].wait_recv()
-        serve(j, True)
-
-    half_owner = per_owner // 2
-    keys_of(0, half_owner)
-    if half_y > 1:
-        arrive(1)
-    keys_of(half_owner, per_owner)
-    for copy in id_copies:
-        copy.wait_recv()
-    for k in range(1, half_y + 1):
-        if k > 1 or half_y == 1:
-            arrive(k)
-        if k == 1:
-            serve_pair(0)
-        else:
-            for j in sorted({k - 1, n_y - k + 1}):
-                serve_pair(j)
-    serve_pair(half_y)
+    def serve(*labels):
+        for j, sibling in labels:
+            for h in range(2):
+                if sibling:
+                    sib_copies[j, h].wait_recv()
+        readers = [at_y(-j, sibling) for j, sibling in labels]
+        results = [
+            attend(q_sib[j] if sibling else q_ring[j], reader)
+            for (j, sibling), reader in zip(labels, readers)
+        ]
+        for (j, sibling), (read, stats) in zip(labels, results):
+            if j == 0 and not sibling:
+                ret_o[st] = read
+                ret_s[st] = stats
+            else:
+                o_send[j * 2 + sibling] = read
+                s_send[j * 2 + sibling] = stats
+        for (j, sibling), reader in zip(labels, readers):
+            if j == 0 and not sibling:
+                continue
+            label = j * 2 + sibling
+            for source, target, send, recv in (
+                (o_send, ret_o, ret_send_sem, ret_recv_sem),
+                (s_send, ret_s, stat_send_sem, stat_recv_sem),
+            ):
+                copy = pltpu.make_async_remote_copy(
+                    source.at[label], target.at[st], send.at[label], recv.at[label],
+                    device_id=(grp, reader, tp), device_id_type=MESH,
+                )
+                copy.start()
+                ret_copies.append(copy)
+
+    for h in range(2):
+        for j, near, far, sign in ((2, 3, 4, 1), (n_y - 2, n_y - 3, 4, -1)):
+            ring_copies[j, h].wait_recv()
+            if h == (0 if sign > 0 else 1):
+                push(j, far, h, 2 * sign)
+            push(j, near, h, sign)
+            across(j, h)
+    for h in range(2):
+        for j in (1, n_y - 1):
+            ring_copies[j, h].wait_recv()
+            across(j, h)
+    serve((1, 0), (n_y - 1, 0))
+    serve((2, 0), (n_y - 2, 0))
+    serve((1, 1), (n_y - 1, 1))
+    serve((2, 1), (n_y - 2, 1))
+    serve((0, 0), (0, 1))
 
     got_wm.wait()
     over_width = ((1,), (1,))
@@ -324,9 +330,19 @@
     for c in range(PIECES):
         part[c] = dot(out_mix[...], wom[:, c * width : (c + 1) * width])
 
+    for h in range(2):
+        for j in (3, n_y - 3):
+            ring_copies[j, h].wait_recv()
+            across(j, h)
+    for h in range(2):
+        ring_copies[4, h].wait_recv()
+        across(4, h)
+    serve((4, 0), (3, 0), (n_y - 3, 0))
+    serve((4, 1), (3, 1), (n_y - 3, 1))
+
     owners, ranks = [], []
     for e in range(blocks * NPB):
-        owner = ids[e // NPB, e % NPB] // per_owner
+        owner = own_ids[e // NPB, e % NPB] // per_owner
         rank = jnp.int32(0)
         for before in owners:
             rank = rank + jnp.where(before == owner, 1, 0)
@@ -433,14 +449,14 @@
     mine_rows = count // n_tp
     hbm = pl.BlockSpec(memory_space=pltpu.HBM)
     vmem = pl.BlockSpec(memory_space=pltpu.VMEM)
-    smem = pl.BlockSpec(memory_space=pltpu.SMEM)
     specs = [hbm] * 15
-    specs[1] = specs[9] = vmem
-    specs[12] = smem
     dma = pltpu.SemaphoreType.DMA
     columns = width // PIECES
     scratch = dict(
         tok=pltpu.VMEM((count, width), BF16),
+        gains=pltpu.VMEM((2, width), F32),
+        own_ids=pltpu.SMEM((blocks, NPB), jnp.int32),
+        slot_of=pltpu.SMEM((n_st, 4), jnp.int32),
         normed=pltpu.VMEM((count, width), BF16),
         wg=pltpu.VMEM((mix_width, width), BF16),
         wm=pltpu.VMEM((mix_width, width), BF16),
@@ -468,7 +484,7 @@
         part=pltpu.VMEM((PIECES, count, columns), F32),
         rs_send=pltpu.VMEM((2, n_tp // 2, PIECES, mine_rows, columns), BF16),
         rs_recv=pltpu.VMEM((2, n_tp // 2, PIECES, mine_rows, columns), BF16),
-        in_sem=dma((11,)),
+        in_sem=dma((14,)),
         row_sem=dma((held,)),
         ids_send_sem=dma((n_st,)),
         ids_recv_sem=dma((n_st,)),

time: 69.5 us -> 68 us (0.978)
  the two profiles are of different devices: /device:TPU:513 before, /device:TPU:528 now
where the time goes in v3:
time: 68 us; the launch traced here: 67.9 us
  Pallas kernels  66.3 us (98%)
  local copies, waits for them, and re-layouts  1.57 us (2%)
    pallas_call x1, Pallas kernels, local(): pl.pallas_call(body, out_shape=jax.ShapeDtypeStruct((mine_rows, width), B...  66.3 us
    unnamed x1, local copies, waits for them, and re-layouts  1.57 us

profile of v3, /device:TPU:528, one launch (start us, length us, event | category | flops | bytes accessed | tf_op | source)
XLA Modules:
  0.0 67.9 jit_solution(8538988841434534468)
XLA Ops:
  0.0 66.3 %layer.1 = bf16[32,2048]{1,0:T(8,128)(2,1)} custom-call(bf16[256,2048]{1,0:T(8,128)(2,1)} %refs_0_.1, f32[2048]{0:T(1024)} %refs_1_.1, bf16[192,2048]{1,0:T(8,128)(2,1)} %bitcast.3, bf16[192,2048]{1,0:T(8,128)(2,1)} %bitcast.4, bf16[1,128,128]{2,1,0:T(8,128)(2,1)} %refs_4_.1, bf16[2048,128]{1,0:T(8,128)(2,1)} %refs_5_.1, bf16[192,2048]{1,0:T(8,128)(2,1)} %bitcast.5, ...), custom_call_target="tpu_custom_call" | custom-call | tf_op jit(solution)/shard_map/layer/pallas_call | solution.py:507
  66.4 1.6 %copy.17 = bf16[32,2048]{1,0:T(8,128)(2,1)} copy(bf16[32,2048]{1,0:T(8,128)(2,1)} %layer.1) | data formatting | bytes 262144

commit v4 on v3

--- a/solution.py
+++ b/solution.py
@@ -13,7 +13,7 @@
 NPB = 4
 PROWS = 128
 NORM_ROWS = 32
-PIECES = 4
+PIECES = 2
 
 MESH = pl.DeviceIdType.MESH
 eps = 1e-06
@@ -92,6 +92,7 @@
     ids_recv_sem,
     ring_send_sem,
     ring_recv_sem,
+    two_recv_sem,
     sib_send_sem,
     sib_recv_sem,
     ret_send_sem,
@@ -157,28 +158,30 @@
 
     pl.semaphore_wait(barrier, len(peers))
 
+    for k in range(1, n_st):
+        pltpu.make_async_remote_copy(
+            own_ids, ids_all.at[st], ids_send_sem, ids_recv_sem,
+            device_id=(grp, lax.rem(st + k, n_st), tp), device_id_type=MESH,
+        ).start()
+
+    def drain(like, sem):
+        pltpu.make_async_copy(like, like, sem).wait()
+
     cut = blocks // 2
-    ring_copies, sib_copies = {}, {}
 
     def push(j, after, h, offset):
         piece = pl.ds(h * cut, cut)
-        copy = pltpu.make_async_remote_copy(
-            q_ring[j].at[piece], q_ring[after].at[piece],
-            ring_send_sem.at[after, h], ring_recv_sem.at[after, h],
+        recv = two_recv_sem.at[after // 4, h] if after in (2, n_y - 2) else ring_recv_sem.at[after]
+        pltpu.make_async_remote_copy(
+            q_ring[j].at[piece], q_ring[after].at[piece], ring_send_sem, recv,
             device_id=(grp, at_y(offset), tp), device_id_type=MESH,
-        )
-        copy.start()
-        ring_copies[after, h] = copy
-
-    def across(j, h):
-        piece = pl.ds(h * cut, cut)
-        copy = pltpu.make_async_remote_copy(
-            q_ring[j].at[piece], q_sib[j].at[piece],
-            sib_send_sem.at[j, h], sib_recv_sem.at[j, h],
+        ).start()
+
+    def across(j):
+        pltpu.make_async_remote_copy(
+            q_ring[j], q_sib[j], sib_send_sem, sib_recv_sem.at[j],
             device_id=(grp, at_y(0, True), tp), device_id_type=MESH,
-        )
-        copy.start()
-        sib_copies[j, h] = copy
+        ).start()
 
     for h in range(2):
         push(0, 2, h, 2)
@@ -186,17 +189,8 @@
     for h in range(2):
         push(0, 1, h, 1)
         push(0, n_y - 1, h, -1)
-    for h in range(2):
-        across(0, h)
-
-    id_copies = []
-    for k in range(1, n_st):
-        copy = pltpu.make_async_remote_copy(
-            own_ids, ids_all.at[st], ids_send_sem.at[k], ids_recv_sem.at[k],
-            device_id=(grp, lax.rem(st + k, n_st), tp), device_id_type=MESH,
-        )
-        copy.start()
-        id_copies.append(copy)
+    across(0)
+
     for b in range(blocks):
         for n in range(NPB):
             ids_all[st, b, n] = own_ids[b, n]
@@ -215,26 +209,6 @@
         return carry
 
     lax.fori_loop(0, per_owner, keys_of, 0)
-
-    for copy in id_copies:
-        copy.wait_recv()
-
-    def slots(reader, carry):
-        p0 = p1 = b0 = b1 = seen = jnp.int32(0)
-        for b in range(blocks):
-            for n in range(NPB):
-                local = ids_all[reader, b, n] - st * per_owner
-                mine = (local >= 0) & (local < per_owner)
-                is0 = mine & (seen == 0)
-                is1 = mine & (seen == 1)
-                p0, b0 = jnp.where(is0, local, p0), jnp.where(is0, b, b0)
-                p1, b1 = jnp.where(is1, local, p1), jnp.where(is1, b, b1)
-                seen = seen + jnp.where(mine, 1, 0)
-        for k, value in enumerate((p0, p1, b0, b1)):
-            slot_of[reader, k] = value
-        return carry
-
-    lax.fori_loop(0, n_st, slots, 0)
 
     lanes = lax.broadcasted_iota(jnp.int32, (1, 2 * RBLOCK), 1)
     first_half = lanes < RBLOCK
@@ -253,13 +227,10 @@
         read = jnp.where(first_half, dot(value_of[p0], weight), dot(value_of[p1], weight))
         return read.astype(BF16), jnp.concatenate([top, total], axis=0)
 
-    ret_copies = []
-
     def serve(*labels):
         for j, sibling in labels:
-            for h in range(2):
-                if sibling:
-                    sib_copies[j, h].wait_recv()
+            if sibling:
+                drain(q_sib[j], sib_recv_sem.at[j])
         readers = [at_y(-j, sibling) for j, sibling in labels]
         results = [
             attend(q_sib[j] if sibling else q_ring[j], reader)
@@ -280,24 +251,42 @@
                 (o_send, ret_o, ret_send_sem, ret_recv_sem),
                 (s_send, ret_s, stat_send_sem, stat_recv_sem),
             ):
-                copy = pltpu.make_async_remote_copy(
-                    source.at[label], target.at[st], send.at[label], recv.at[label],
+                pltpu.make_async_remote_copy(
+                    source.at[label], target.at[st], send, recv,
                     device_id=(grp, reader, tp), device_id_type=MESH,
-                )
-                copy.start()
-                ret_copies.append(copy)
+                ).start()
 
     for h in range(2):
         for j, near, far, sign in ((2, 3, 4, 1), (n_y - 2, n_y - 3, 4, -1)):
-            ring_copies[j, h].wait_recv()
+            drain(q_ring[j].at[pl.ds(h * cut, cut)], two_recv_sem.at[j // 4, h])
             if h == (0 if sign > 0 else 1):
                 push(j, far, h, 2 * sign)
             push(j, near, h, sign)
-            across(j, h)
-    for h in range(2):
-        for j in (1, n_y - 1):
-            ring_copies[j, h].wait_recv()
-            across(j, h)
+    for j in (1, n_y - 1):
+        drain(q_ring[j], ring_recv_sem.at[j])
+        across(j)
+    for j in (2, n_y - 2):
+        across(j)
+
+    drain(ids_all.at[pl.ds(0, n_st - 1)], ids_recv_sem)
+
+    def slots(reader, carry):
+        p0 = p1 = b0 = b1 = seen = jnp.int32(0)
+        for b in range(blocks):
+            for n in range(NPB):
+                local = ids_all[reader, b, n] - st * per_owner
+                mine = (local >= 0) & (local < per_owner)
+                is0 = mine & (seen == 0)
+                is1 = mine & (seen == 1)
+                p0, b0 = jnp.where(is0, local, p0), jnp.where(is0, b, b0)
+                p1, b1 = jnp.where(is1, local, p1), jnp.where(is1, b, b1)
+                seen = seen + jnp.where(mine, 1, 0)
+        for k, value in enumerate((p0, p1, b0, b1)):
+            slot_of[reader, k] = value
+        return carry
+
+    lax.fori_loop(0, n_st, slots, 0)
+
     serve((1, 0), (n_y - 1, 0))
     serve((2, 0), (n_y - 2, 0))
     serve((1, 1), (n_y - 1, 1))
@@ -330,13 +319,9 @@
     for c in range(PIECES):
         part[c] = dot(out_mix[...], wom[:, c * width : (c + 1) * width])
 
-    for h in range(2):
-        for j in (3, n_y - 3):
-            ring_copies[j, h].wait_recv()
-            across(j, h)
-    for h in range(2):
-        ring_copies[4, h].wait_recv()
-        across(4, h)
+    for j in (3, n_y - 3, 4):
+        drain(q_ring[j], ring_recv_sem.at[j])
+        across(j)
     serve((4, 0), (3, 0), (n_y - 3, 0))
     serve((4, 1), (3, 1), (n_y - 3, 1))
 
@@ -348,8 +333,8 @@
             rank = rank + jnp.where(before == owner, 1, 0)
         owners.append(owner)
         ranks.append(rank)
-    for copy in ret_copies:
-        copy.wait_recv()
+    drain(ret_o.at[pl.ds(0, n_st - 1)], ret_recv_sem)
+    drain(ret_s.at[pl.ds(0, n_st - 1)], stat_recv_sem)
     got_wor.wait()
     for pair in range(blocks // 2):
         tops, totals, reads = [], [], []
@@ -386,25 +371,25 @@
         start = pl.multiple_of(target * mine_rows + lo, mine_rows // 2)
         value = part[c, pl.ds(start, size), :]
         if k == half_tp:
-            rs_send[d, k - 1, c, lo : lo + size, :] = value.astype(BF16)
+            rs_send[k - 1, d, c, lo : lo + size, :] = value.astype(BF16)
         else:
             rs_copies[c, d, k + 1].wait_recv()
             if k + 1 == half_tp:
                 cut_rows = mine_rows // 2
                 low = d * cut_rows
-                rs_send[d, k - 1, c, low : low + cut_rows, :] = (
+                rs_send[k - 1, d, c, low : low + cut_rows, :] = (
                     part[c, pl.ds(pl.multiple_of(target * mine_rows + low, cut_rows), cut_rows), :]
-                    + rs_recv[d, k, c, low : low + cut_rows, :].astype(F32)
+                    + rs_recv[k, d, c, low : low + cut_rows, :].astype(F32)
                 ).astype(BF16)
                 other = cut_rows - low
-                rs_send[d, k - 1, c, other : other + cut_rows, :] = part[
+                rs_send[k - 1, d, c, other : other + cut_rows, :] = part[
                     c, pl.ds(pl.multiple_of(target * mine_rows + other, cut_rows), cut_rows), :
                 ].astype(BF16)
             else:
-                rs_send[d, k - 1, c] = (value + rs_recv[d, k, c].astype(F32)).astype(BF16)
+                rs_send[k - 1, d, c] = (value + rs_recv[k, d, c].astype(F32)).astype(BF16)
         copy = pltpu.make_async_remote_copy(
-            rs_send.at[d, k - 1, c, pl.ds(lo, size)], rs_recv.at[d, k - 1, c, pl.ds(lo, size)],
-            rs_send_sem.at[d, k - 1, c], rs_recv_sem.at[d, k - 1, c],
+            rs_send.at[k - 1, d, c, pl.ds(lo, size)], rs_recv.at[k - 1, d, c, pl.ds(lo, size)],
+            rs_send_sem.at[k // half_tp], rs_recv_sem.at[k - 1, d, c],
             device_id=(grp, st, along_tp(sign)), device_id_type=MESH,
         )
         copy.start()
@@ -425,17 +410,20 @@
         if half_tp == 1:
             cut_rows = mine_rows // 2
             both = jnp.concatenate(
-                [rs_recv[0, 0, c, :cut_rows, :], rs_recv[1, 0, c, cut_rows:, :]], axis=0
+                [rs_recv[0, 0, c, :cut_rows, :], rs_recv[0, 1, c, cut_rows:, :]], axis=0
             ).astype(F32)
         else:
-            both = rs_recv[0, 0, c].astype(F32) + rs_recv[1, 0, c].astype(F32)
+            both = rs_recv[0, 0, c].astype(F32) + rs_recv[0, 1, c].astype(F32)
         out[:, c * width : (c + 1) * width] = (part[c, here, :] + both).astype(BF16)
 
-    for copy in (
-        id_copies + list(ring_copies.values()) + list(sib_copies.values())
-        + ret_copies + list(rs_copies.values())
-    ):
-        copy.wait_send()
+    drain(ids_all.at[pl.ds(0, n_st - 1)], ids_send_sem)
+    drain(o_send.at[pl.ds(0, 2 * (n_y - 1))], ring_send_sem)
+    drain(o_send, sib_send_sem)
+    drain(o_send.at[pl.ds(0, n_st - 1)], ret_send_sem)
+    drain(s_send.at[pl.ds(0, n_st - 1)], stat_send_sem)
+    drain(rs_send.at[half_tp - 1, 0], rs_send_sem.at[1])
+    if half_tp > 1:
+        drain(rs_send.at[pl.ds(0, half_tp - 1)], rs_send_sem.at[0])
 
 
 def local(*args, n_st, n_tp):
@@ -482,22 +470,23 @@
         out_mix=pltpu.VMEM((count, mix_width), BF16),
         out_read=pltpu.VMEM((count, HD), BF16),
         part=pltpu.VMEM((PIECES, count, columns), F32),
-        rs_send=pltpu.VMEM((2, n_tp // 2, PIECES, mine_rows, columns), BF16),
-        rs_recv=pltpu.VMEM((2, n_tp // 2, PIECES, mine_rows, columns), BF16),
+        rs_send=pltpu.VMEM((n_tp // 2, 2, PIECES, mine_rows, columns), BF16),
+        rs_recv=pltpu.VMEM((n_tp // 2, 2, PIECES, mine_rows, columns), BF16),
         in_sem=dma((14,)),
         row_sem=dma((held,)),
-        ids_send_sem=dma((n_st,)),
-        ids_recv_sem=dma((n_st,)),
-        ring_send_sem=dma((n_y, 2)),
-        ring_recv_sem=dma((n_y, 2)),
-        sib_send_sem=dma((n_y, 2)),
-        sib_recv_sem=dma((n_y, 2)),
-        ret_send_sem=dma((n_st,)),
-        ret_recv_sem=dma((n_st,)),
-        stat_send_sem=dma((n_st,)),
-        stat_recv_sem=dma((n_st,)),
-        rs_send_sem=dma((2, n_tp // 2, PIECES)),
-        rs_recv_sem=dma((2, n_tp // 2, PIECES)),
+        ids_send_sem=dma,
+        ids_recv_sem=dma,
+        ring_send_sem=dma,
+        ring_recv_sem=dma((n_y,)),
+        two_recv_sem=dma((2, 2)),
+        sib_send_sem=dma,
+        sib_recv_sem=dma((n_y,)),
+        ret_send_sem=dma,
+        ret_recv_sem=dma,
+        stat_send_sem=dma,
+        stat_recv_sem=dma,
+        rs_send_sem=dma((2,)),
+        rs_recv_sem=dma((n_tp // 2, 2, PIECES)),
     )
     names = list(scratch)
 

time: 68 us -> 65.7 us (0.966)
  Pallas kernels: 66.3 us -> 64 us
    pallas_call x1, Pallas kernels: 66.3 us -> 64 us  [local(): pl.pallas_call(body, out_shape=jax.ShapeDtypeStruct((mine_rows, width), B...]
where the time goes in v4:
time: 65.7 us; the launch traced here: 65.5 us
  Pallas kernels  64 us (97%)
  local copies, waits for them, and re-layouts  1.57 us (2%)
    pallas_call x1, Pallas kernels, local(): pl.pallas_call(body, out_shape=jax.ShapeDtypeStruct((mine_rows, width), B...  64 us
    unnamed x1, local copies, waits for them, and re-layouts  1.57 us

profile of v4, /device:TPU:528, one launch (start us, length us, event | category | flops | bytes accessed | tf_op | source)
XLA Modules:
  0.0 65.5 jit_solution(6335162123569607384)
XLA Ops:
  0.0 64.0 %layer.1 = bf16[32,2048]{1,0:T(8,128)(2,1)} custom-call(bf16[256,2048]{1,0:T(8,128)(2,1)} %refs_0_.1, f32[2048]{0:T(1024)} %refs_1_.1, bf16[192,2048]{1,0:T(8,128)(2,1)} %bitcast.3, bf16[192,2048]{1,0:T(8,128)(2,1)} %bitcast.4, bf16[1,128,128]{2,1,0:T(8,128)(2,1)} %refs_4_.1, bf16[2048,128]{1,0:T(8,128)(2,1)} %refs_5_.1, bf16[192,2048]{1,0:T(8,128)(2,1)} %bitcast.5, ...), custom_call_target="tpu_custom_call" | custom-call | tf_op jit(solution)/shard_map/layer/pallas_call | solution.py:496
  64.0 1.6 %copy.17 = bf16[32,2048]{1,0:T(8,128)(2,1)} copy(bf16[32,2048]{1,0:T(8,128)(2,1)} %layer.1) | data formatting | bytes 262144

commit v5 on v4

--- a/solution.py
+++ b/solution.py
@@ -185,10 +185,10 @@
 
     for h in range(2):
         push(0, 2, h, 2)
-        push(0, n_y - 2, h, -2)
+        push(0, n_y - 2, 1 - h, -2)
     for h in range(2):
         push(0, 1, h, 1)
-        push(0, n_y - 1, h, -1)
+        push(0, n_y - 1, 1 - h, -1)
     across(0)
 
     for b in range(blocks):
@@ -256,17 +256,14 @@
                     device_id=(grp, reader, tp), device_id_type=MESH,
                 ).start()
 
-    for h in range(2):
-        for j, near, far, sign in ((2, 3, 4, 1), (n_y - 2, n_y - 3, 4, -1)):
+    def forward(i):
+        for j, near, h, sign in ((2, 3, i, 1), (n_y - 2, n_y - 3, 1 - i, -1)):
             drain(q_ring[j].at[pl.ds(h * cut, cut)], two_recv_sem.at[j // 4, h])
-            if h == (0 if sign > 0 else 1):
-                push(j, far, h, 2 * sign)
+            if i == 0:
+                push(j, 4, h, 2 * sign)
             push(j, near, h, sign)
-    for j in (1, n_y - 1):
-        drain(q_ring[j], ring_recv_sem.at[j])
-        across(j)
-    for j in (2, n_y - 2):
-        across(j)
+
+    forward(0)
 
     drain(ids_all.at[pl.ds(0, n_st - 1)], ids_recv_sem)
 
@@ -285,12 +282,25 @@
             slot_of[reader, k] = value
         return carry
 
-    lax.fori_loop(0, n_st, slots, 0)
+    lax.fori_loop(0, n_st, slots, 0, unroll=4)
+
+    forward(1)
+    for j in (1, n_y - 1):
+        drain(q_ring[j], ring_recv_sem.at[j])
+        across(j)
+    for j in (2, n_y - 2):
+        across(j)
 
     serve((1, 0), (n_y - 1, 0))
     serve((2, 0), (n_y - 2, 0))
     serve((1, 1), (n_y - 1, 1))
     serve((2, 1), (n_y - 2, 1))
+
+    for j in (3, n_y - 3, 4):
+        drain(q_ring[j], ring_recv_sem.at[j])
+        across(j)
+    serve((4, 0), (3, 0), (n_y - 3, 0))
+    serve((4, 1), (3, 1), (n_y - 3, 1))
     serve((0, 0), (0, 1))
 
     got_wm.wait()
@@ -318,12 +328,6 @@
     width = part.shape[2]
     for c in range(PIECES):
         part[c] = dot(out_mix[...], wom[:, c * width : (c + 1) * width])
-
-    for j in (3, n_y - 3, 4):
-        drain(q_ring[j], ring_recv_sem.at[j])
-        across(j)
-    serve((4, 0), (3, 0), (n_y - 3, 0))
-    serve((4, 1), (3, 1), (n_y - 3, 1))
 
     owners, ranks = [], []
     for e in range(blocks * NPB):

time: 65.7 us -> 63.4 us (0.965)
  Pallas kernels: 64 us -> 61.4 us
    pallas_call x1, Pallas kernels: 64 us -> 61.4 us  [local(): pl.pallas_call(body, out_shape=jax.ShapeDtypeStruct((mine_rows, width), B...]
where the time goes in v5:
time: 63.4 us; the launch traced here: 63 us
  Pallas kernels  61.4 us (97%)
  local copies, waits for them, and re-layouts  1.57 us (2%)
    pallas_call x1, Pallas kernels, local(): pl.pallas_call(body, out_shape=jax.ShapeDtypeStruct((mine_rows, width), B...  61.4 us
    unnamed x1, local copies, waits for them, and re-layouts  1.57 us

profile of v5, /device:TPU:528, one launch (start us, length us, event | category | flops | bytes accessed | tf_op | source)
XLA Modules:
  0.0 63.0 jit_solution(14538288713448723198)
XLA Ops:
  0.0 61.4 %layer.1 = bf16[32,2048]{1,0:T(8,128)(2,1)} custom-call(bf16[256,2048]{1,0:T(8,128)(2,1)} %refs_0_.1, f32[2048]{0:T(1024)} %refs_1_.1, bf16[192,2048]{1,0:T(8,128)(2,1)} %bitcast.3, bf16[192,2048]{1,0:T(8,128)(2,1)} %bitcast.4, bf16[1,128,128]{2,1,0:T(8,128)(2,1)} %refs_4_.1, bf16[2048,128]{1,0:T(8,128)(2,1)} %refs_5_.1, bf16[192,2048]{1,0:T(8,128)(2,1)} %bitcast.5, ...), custom_call_target="tpu_custom_call" | custom-call | tf_op jit(solution)/shard_map/layer/pallas_call | solution.py:500
  61.4 1.6 %copy.17 = bf16[32,2048]{1,0:T(8,128)(2,1)} copy(bf16[32,2048]{1,0:T(8,128)(2,1)} %layer.1) | data formatting | bytes 262144

commit v6 on v5

--- a/solution.py
+++ b/solution.py
@@ -499,12 +499,12 @@
 
     return pl.pallas_call(
         body,
-        out_shape=jax.ShapeDtypeStruct((mine_rows, width), BF16),
+        out_shape=pltpu.VMEM((mine_rows, width), BF16),
         in_specs=specs,
         out_specs=vmem,
         scratch_shapes=list(scratch.values()),
         compiler_params=pltpu.CompilerParams(
-            collective_id=0, has_side_effects=True, vmem_limit_bytes=67_000_000
+            collective_id=0, has_side_effects=True, vmem_limit_bytes=66_800_000
         ),
         name="layer",
     )(*args)

time: 63.4 us -> 61.8 us (0.975)
  local copies, waits for them, and re-layouts: 1.57 us -> 0.66 us
  Pallas kernels: 61.4 us -> 60.7 us
    unnamed x1, local copies, waits for them, and re-layouts: 1.57 us -> 0.66 us
    pallas_call x1, Pallas kernels: 61.4 us -> 60.7 us  [local(): pl.pallas_call(body, out_shape=pltpu.VMEM((mine_rows, width), BF16), in_s...]
where the time goes in v6:
time: 61.8 us; the launch traced here: 61.4 us
  Pallas kernels  60.7 us (98%)
  local copies, waits for them, and re-layouts  0.66 us (1%)
    pallas_call x1, Pallas kernels, local(): pl.pallas_call(body, out_shape=pltpu.VMEM((mine_rows, width), BF16), in_s...  60.7 us

profile of v6, /device:TPU:528, one launch (start us, length us, event | category | flops | bytes accessed | tf_op | source)
XLA Modules:
  0.0 61.4 jit_solution(7160494594319350922)
XLA Ops:
  0.0 60.7 %layer.1 = bf16[32,2048]{1,0:T(8,128)(2,1)S(1)} custom-call(bf16[256,2048]{1,0:T(8,128)(2,1)} %refs_0_.1, f32[2048]{0:T(1024)} %refs_1_.1, bf16[192,2048]{1,0:T(8,128)(2,1)} %bitcast.3, bf16[192,2048]{1,0:T(8,128)(2,1)} %bitcast.4, bf16[1,128,128]{2,1,0:T(8,128)(2,1)} %refs_4_.1, bf16[2048,128]{1,0:T(8,128)(2,1)} %refs_5_.1, bf16[192,2048]{1,0:T(8,128)(2,1)} %bitcast.5, ...), custom_call_target="tpu_custom_call" | custom-call | tf_op jit(solution)/shard_map/layer/pallas_call | solution.py:500
  60.7 0.7 %copy.17 = bf16[32,2048]{1,0:T(8,128)(2,1)} copy(bf16[32,2048]{1,0:T(8,128)(2,1)S(1)} %layer.1) | data formatting | bytes 262144

commit v7 on v6

--- a/solution.py
+++ b/solution.py
@@ -25,15 +25,11 @@
     return lax.dot_general(a, b, (dims, ((), ())), preferred_element_type=F32)
 
 
-def row_norm(source, gain, target, rows):
-    def some(i, carry):
-        at = pl.ds(pl.multiple_of(i * NORM_ROWS, NORM_ROWS), NORM_ROWS)
-        wide = source[at, :].astype(F32)
+def row_norm(source, gain, target, low, high):
+    for at in range(low, high, NORM_ROWS):
+        wide = source[at : at + NORM_ROWS, :].astype(F32)
         scale = lax.rsqrt(jnp.mean(wide * wide, axis=-1, keepdims=True) + eps)
-        target[at, :] = (wide * scale * gain).astype(BF16)
-        return carry
-
-    lax.fori_loop(0, rows // NORM_ROWS, some, 0)
+        target[at : at + NORM_ROWS, :] = (wide * scale * gain).astype(BF16)
 
 
 def kernel(
@@ -70,7 +66,8 @@
     wom,
     wor,
     rows_in,
-    rows_norm,
+    norm_even,
+    norm_odd,
     key_of,
     value_of,
     q_ring,
@@ -150,10 +147,14 @@
 
     got_pre.wait()
     got_tok.wait()
-    row_norm(tok, gains[0].reshape(1, -1), normed, count)
     got_wq.wait()
-    own_q = dot(normed[...], wq[...]).astype(BF16)
-    q_ring[0][...] = own_q.reshape(blocks, RBLOCK, HD)
+    cut = blocks // 2
+    half = cut * RBLOCK
+    for h in range(2):
+        rows = slice(h * half, (h + 1) * half)
+        row_norm(tok, gains[0].reshape(1, -1), normed, h * half, (h + 1) * half)
+        own_q = dot(normed[rows, :], wq[...]).astype(BF16)
+        q_ring[0][h * cut : (h + 1) * cut] = own_q.reshape(cut, RBLOCK, HD)
     got_ids.wait()
 
     pl.semaphore_wait(barrier, len(peers))
@@ -166,8 +167,6 @@
 
     def drain(like, sem):
         pltpu.make_async_copy(like, like, sem).wait()
-
-    cut = blocks // 2
 
     def push(j, after, h, offset):
         piece = pl.ds(h * cut, cut)
@@ -200,15 +199,34 @@
     got_mem.wait()
     mem_row = gains[1].reshape(1, -1)
 
-    def keys_of(p, carry):
-        pltpu.make_async_copy(store.at[p], rows_in.at[p], row_sem.at[p]).wait()
-        row_norm(rows_in.at[p], mem_row, rows_norm, PROWS)
-        both = dot(rows_norm[...], wkv[...])
+    def norm_of(p, target):
+        row_norm(rows_in.at[p], mem_row, target, 0, PROWS)
+
+    def keys_of(p, source):
+        both = dot(source[...], wkv[...])
         key_of[p] = both[:, :HD].astype(BF16)
         value_of[p] = jnp.transpose(both[:, HD:]).astype(BF16)
+
+    def row_wait(p):
+        pltpu.make_async_copy(store.at[p], rows_in.at[p], row_sem.at[p]).wait()
+
+    row_wait(0)
+    norm_of(0, norm_even)
+
+    def two(i, carry):
+        row_wait(2 * i + 1)
+        row_wait(2 * i + 2)
+        keys_of(2 * i, norm_even)
+        norm_of(2 * i + 1, norm_odd)
+        keys_of(2 * i + 1, norm_odd)
+        norm_of(2 * i + 2, norm_even)
         return carry
 
-    lax.fori_loop(0, per_owner, keys_of, 0)
+    lax.fori_loop(0, per_owner // 2 - 1, two, 0)
+    row_wait(per_owner - 1)
+    keys_of(per_owner - 2, norm_even)
+    norm_of(per_owner - 1, norm_odd)
+    keys_of(per_owner - 1, norm_odd)
 
     lanes = lax.broadcasted_iota(jnp.int32, (1, 2 * RBLOCK), 1)
     first_half = lanes < RBLOCK
@@ -460,7 +478,8 @@
         wom=pltpu.VMEM((mix_width, width), BF16),
         wor=pltpu.VMEM((HD, width), BF16),
         rows_in=pltpu.VMEM((held, PROWS, width), BF16),
-        rows_norm=pltpu.VMEM((PROWS, width), BF16),
+        norm_even=pltpu.VMEM((PROWS, width), BF16),
+        norm_odd=pltpu.VMEM((PROWS, width), BF16),
         key_of=pltpu.VMEM((held, PROWS, HD), BF16),
         value_of=pltpu.VMEM((held, HD, PROWS), BF16),
         q_ring=[pltpu.VMEM((blocks, RBLOCK, HD), BF16) for _ in range(n_y)],

time: 61.8 us -> 59.8 us (0.968)
  Pallas kernels: 60.7 us -> 59 us
    pallas_call x1, Pallas kernels: 60.7 us -> 59 us  [local(): pl.pallas_call(body, out_shape=pltpu.VMEM((mine_rows, width), BF16), in_s...]
where the time goes in v7:
time: 59.8 us; the launch traced here: 59.6 us
  Pallas kernels  59 us (99%)
  local copies, waits for them, and re-layouts  0.66 us (1%)
    pallas_call x1, Pallas kernels, local(): pl.pallas_call(body, out_shape=pltpu.VMEM((mine_rows, width), BF16), in_s...  59 us

profile of v7, /device:TPU:528, one launch (start us, length us, event | category | flops | bytes accessed | tf_op | source)
XLA Modules:
  0.0 59.6 jit_solution(11001912303143833602)
XLA Ops:
  0.0 59.0 %layer.1 = bf16[32,2048]{1,0:T(8,128)(2,1)S(1)} custom-call(bf16[256,2048]{1,0:T(8,128)(2,1)} %refs_0_.1, f32[2048]{0:T(1024)} %refs_1_.1, bf16[192,2048]{1,0:T(8,128)(2,1)} %bitcast.3, bf16[192,2048]{1,0:T(8,128)(2,1)} %bitcast.4, bf16[1,128,128]{2,1,0:T(8,128)(2,1)} %refs_4_.1, bf16[2048,128]{1,0:T(8,128)(2,1)} %refs_5_.1, bf16[192,2048]{1,0:T(8,128)(2,1)} %bitcast.5, ...), custom_call_target="tpu_custom_call" | custom-call | tf_op jit(solution)/shard_map/layer/pallas_call | solution.py:519
  59.0 0.7 %copy.17 = bf16[32,2048]{1,0:T(8,128)(2,1)} copy(bf16[32,2048]{1,0:T(8,128)(2,1)S(1)} %layer.1) | data formatting | bytes 262144

commit v8 on v7

--- a/solution.py
+++ b/solution.py
@@ -286,18 +286,21 @@
     drain(ids_all.at[pl.ds(0, n_st - 1)], ids_recv_sem)
 
     def slots(reader, carry):
-        p0 = p1 = b0 = b1 = seen = jnp.int32(0)
+        first = last = jnp.int32(0)
+        codes = []
         for b in range(blocks):
             for n in range(NPB):
                 local = ids_all[reader, b, n] - st * per_owner
                 mine = (local >= 0) & (local < per_owner)
-                is0 = mine & (seen == 0)
-                is1 = mine & (seen == 1)
-                p0, b0 = jnp.where(is0, local, p0), jnp.where(is0, b, b0)
-                p1, b1 = jnp.where(is1, local, p1), jnp.where(is1, b, b1)
-                seen = seen + jnp.where(mine, 1, 0)
-        for k, value in enumerate((p0, p1, b0, b1)):
-            slot_of[reader, k] = value
+                code = local * blocks + b
+                last = jnp.where(mine, code, last)
+                codes.append((mine, code))
+        for mine, code in reversed(codes):
+            first = jnp.where(mine, code, first)
+        slot_of[reader, 0] = first // blocks
+        slot_of[reader, 1] = last // blocks
+        slot_of[reader, 2] = lax.rem(first, blocks)
+        slot_of[reader, 3] = lax.rem(last, blocks)
         return carry
 
     lax.fori_loop(0, n_st, slots, 0, unroll=4)
@@ -309,10 +312,8 @@
     for j in (2, n_y - 2):
         across(j)
 
-    serve((1, 0), (n_y - 1, 0))
-    serve((2, 0), (n_y - 2, 0))
-    serve((1, 1), (n_y - 1, 1))
-    serve((2, 1), (n_y - 2, 1))
+    serve((1, 0), (n_y - 1, 0), (2, 0), (n_y - 2, 0))
+    serve((1, 1), (n_y - 1, 1), (2, 1), (n_y - 2, 1))
 
     for j in (3, n_y - 3, 4):
         drain(q_ring[j], ring_recv_sem.at[j])
@@ -393,7 +394,8 @@
         start = pl.multiple_of(target * mine_rows + lo, mine_rows // 2)
         value = part[c, pl.ds(start, size), :]
         if k == half_tp:
-            rs_send[k - 1, d, c, lo : lo + size, :] = value.astype(BF16)
+            added = first[lo : lo + size, c * width : (c + 1) * width]
+            rs_send[k - 1, d, c, lo : lo + size, :] = (value + added).astype(BF16)
         else:
             rs_copies[c, d, k + 1].wait_recv()
             if k + 1 == half_tp:
@@ -417,10 +419,13 @@
         copy.start()
         rs_copies[c, d, k] = copy
 
+    start = pl.multiple_of(along_tp(half_tp) * mine_rows, mine_rows)
+    first = dot(out_read[pl.ds(start, mine_rows), :], wor[...])
+    for c in range(PIECES):
+        for d in range(2):
+            pass_on(c, d, half_tp)
     for c in range(PIECES):
         part[c] = part[c] + dot(out_read[...], wor[:, c * width : (c + 1) * width])
-        for d in range(2):
-            pass_on(c, d, half_tp)
     for k in range(half_tp - 1, 0, -1):
         for c in range(PIECES):
             for d in range(2):

time: 59.8 us -> 59.4 us (level)
  Pallas kernels: 59 us -> 58.1 us
    pallas_call x1, Pallas kernels: 59 us -> 58.1 us  [local(): pl.pallas_call(body, out_shape=pltpu.VMEM((mine_rows, width), BF16), in_s...]
where the time goes in v8:
time: 59.4 us; the launch traced here: 58.8 us
  Pallas kernels  58.1 us (98%)
  local copies, waits for them, and re-layouts  0.66 us (1%)
    pallas_call x1, Pallas kernels, local(): pl.pallas_call(body, out_shape=pltpu.VMEM((mine_rows, width), BF16), in_s...  58.1 us

profile of v8, /device:TPU:528, one launch (start us, length us, event | category | flops | bytes accessed | tf_op | source)
XLA Modules:
  0.0 58.8 jit_solution(9103641281799818475)
XLA Ops:
  0.0 58.1 %layer.1 = bf16[32,2048]{1,0:T(8,128)(2,1)S(1)} custom-call(bf16[256,2048]{1,0:T(8,128)(2,1)} %refs_0_.1, f32[2048]{0:T(1024)} %refs_1_.1, bf16[192,2048]{1,0:T(8,128)(2,1)} %bitcast.3, bf16[192,2048]{1,0:T(8,128)(2,1)} %bitcast.4, bf16[1,128,128]{2,1,0:T(8,128)(2,1)} %refs_4_.1, bf16[2048,128]{1,0:T(8,128)(2,1)} %refs_5_.1, bf16[192,2048]{1,0:T(8,128)(2,1)} %bitcast.5, ...), custom_call_target="tpu_custom_call" | custom-call | tf_op jit(solution)/shard_map/layer/pallas_call | solution.py:524
  58.1 0.7 %copy.17 = bf16[32,2048]{1,0:T(8,128)(2,1)} copy(bf16[32,2048]{1,0:T(8,128)(2,1)S(1)} %layer.1) | data formatting | bytes 262144

commit v9 on v8

--- a/solution.py
+++ b/solution.py
@@ -261,14 +261,14 @@
             else:
                 o_send[j * 2 + sibling] = read
                 s_send[j * 2 + sibling] = stats
-        for (j, sibling), reader in zip(labels, readers):
-            if j == 0 and not sibling:
-                continue
-            label = j * 2 + sibling
-            for source, target, send, recv in (
-                (o_send, ret_o, ret_send_sem, ret_recv_sem),
-                (s_send, ret_s, stat_send_sem, stat_recv_sem),
-            ):
+        for source, target, send, recv in (
+            (o_send, ret_o, ret_send_sem, ret_recv_sem),
+            (s_send, ret_s, stat_send_sem, stat_recv_sem),
+        ):
+            for (j, sibling), reader in zip(labels, readers):
+                if j == 0 and not sibling:
+                    continue
+                label = j * 2 + sibling
                 pltpu.make_async_remote_copy(
                     source.at[label], target.at[st], send, recv,
                     device_id=(grp, reader, tp), device_id_type=MESH,

time: 59.4 us -> 59.8 us (level)
  Pallas kernels: 58.1 us -> 59 us
    pallas_call x1, Pallas kernels: 58.1 us -> 59 us  [local(): pl.pallas_call(body, out_shape=pltpu.VMEM((mine_rows, width), BF16), in_s...]
where the time goes in v9:
time: 59.8 us; the launch traced here: 59.7 us
  Pallas kernels  59 us (99%)
  local copies, waits for them, and re-layouts  0.66 us (1%)
    pallas_call x1, Pallas kernels, local(): pl.pallas_call(body, out_shape=pltpu.VMEM((mine_rows, width), BF16), in_s...  59 us

profile of v9, /device:TPU:528, one launch (start us, length us, event | category | flops | bytes accessed | tf_op | source)
XLA Modules:
  0.0 59.7 jit_solution(5721611214705072776)
XLA Ops:
  0.0 59.0 %layer.1 = bf16[32,2048]{1,0:T(8,128)(2,1)S(1)} custom-call(bf16[256,2048]{1,0:T(8,128)(2,1)} %refs_0_.1, f32[2048]{0:T(1024)} %refs_1_.1, bf16[192,2048]{1,0:T(8,128)(2,1)} %bitcast.3, bf16[192,2048]{1,0:T(8,128)(2,1)} %bitcast.4, bf16[1,128,128]{2,1,0:T(8,128)(2,1)} %refs_4_.1, bf16[2048,128]{1,0:T(8,128)(2,1)} %refs_5_.1, bf16[192,2048]{1,0:T(8,128)(2,1)} %bitcast.5, ...), custom_call_target="tpu_custom_call" | custom-call | tf_op jit(solution)/shard_map/layer/pallas_call | solution.py:524
  59.0 0.7 %copy.17 = bf16[32,2048]{1,0:T(8,128)(2,1)} copy(bf16[32,2048]{1,0:T(8,128)(2,1)S(1)} %layer.1) | data formatting | bytes 262144
